TPU v7x, 256 devices: a whole 4x4x8 slice. The times are simulated.
256 devices in a mesh: ep: 64 (over z, y, core), tp: 4 (over x).
Axes of the slice: x: 4, y: 4, z: 8, core: 2. Of those that a mesh axis runs over, the one named last changes fastest.
Arguments:
- first_input: bfloat16 [32768, 2048], P('ep'), may hold values from -120 to 120
- first_gain: bfloat16 [2048], replicated, may hold values from 0.099609375 to 1.8984375
- pool_inward: bfloat16 [2048, 1024], P(None, 'tp'), may hold values from -0.125 to 0.125
- pool_mixing: bfloat16 [4, 256, 256], P('tp'), may hold values from -0.375 to 0.375
- pool_scale: bfloat16 [1024], P('tp'), may hold values from 0.099609375 to 1.8984375
- pool_outward: bfloat16 [1024, 2048], P('tp'), may hold values from -0.1875 to 0.1875
- second_input: bfloat16 [16384, 2048], P('ep'), may hold values from -120 to 120
- second_gain: bfloat16 [2048], replicated, may hold values from 0.099609375 to 1.8984375
- route_ids: int32 [16384, 2], P('ep'), may hold values from 0 to 31, all different within a row; in each aligned block of 256 rows (0 to 255, 256 to 511, ...) at most 18 rows name the same one
- route_logits: float32 [16384, 2], P('ep'), may hold values from -6 to 6
- expert_gate: bfloat16 [64, 2048, 2048], P('ep', None, 'tp'), may hold values from -0.125 to 0.125
- expert_up: bfloat16 [64, 2048, 2048], P('ep', None, 'tp'), may hold values from -0.125 to 0.125
- expert_down: bfloat16 [64, 2048, 2048], P('ep', 'tp'), may hold values from -0.09375 to 0.09375
Outputs:
- first_out: bfloat16 [32768, 2048], P('ep', 'tp')
- second_out: bfloat16 [16384, 2048], P('ep', 'tp')
Inputs may be any that keep to these rules, and one draw needn't show every extreme that they name: `route_ids`: each row names two different experts. In each aligned block of 256 rows (the rows of one index of ep) no expert is named by more than 18 rows, and in some blocks one expert is named by exactly 18 rows.
All inputs are finite; a program needn't handle non-finite values.
Results may differ from a plain program's by a relative error of at most 0.012.
Values may be sent and summed in bfloat16 or wider, within the bound.
No kernel may reach another device: no remote copies, remote signals or barrier semaphores. Data moves between devices by JAX's collectives and lax.ppermute only.
A program may use at most 64 MiB of HBM per device.

v0:
```python
import functools

import jax
import jax.numpy as jnp
from jax import lax
from jax.experimental import pallas as pl
from jax.experimental.pallas import tpu as pltpu
from jax.sharding import Mesh, PartitionSpec as P

epsilon = 1e-06
EP = ("z", "y", "core")
ZY = ("z", "y")
LANES = 128
MAIN = 16
HALO = 16
f32 = jnp.float32
bf16 = jnp.bfloat16


def shifted(value, axis, steps):
    count = lax.axis_size(axis)
    return lax.ppermute(value, axis, [(i, (i + steps) % count) for i in range(count)])


def from_behind(value, axis, steps):
    count = lax.axis_size(axis)
    leading, last = (max(0, -steps), min(count, count - steps))
    return lax.ppermute(value, axis, [(source, source + steps) for source in range(leading, last)])


def iota(shape, dim):
    return lax.broadcasted_iota(jnp.int32, shape, dim)


def dot(a, b):
    return jnp.dot(a, b, preferred_element_type=f32)


def head_kernel(part_ref, x_ref, gain_ref, ids_ref, out_ref):
    tokens, width = x_ref.shape
    experts = out_ref.shape[0]
    quarter = width // 4
    total = jnp.zeros((tokens, 1), f32)
    for lower in range(0, width, quarter):
        piece = x_ref[:, lower : lower + quarter].astype(f32)
        total = total + jnp.sum(piece * piece, axis=1, keepdims=True)
    inverse = lax.rsqrt(total / width + epsilon)
    start = pl.multiple_of(part_ref[0] * quarter, quarter)
    mine = x_ref[:, pl.ds(start, quarter)].astype(f32)
    normed = (mine * inverse * gain_ref[:, pl.ds(start, quarter)].astype(f32)).astype(bf16)
    named = iota((experts, tokens), 0)
    member = (ids_ref[0:1, :] == named) | (ids_ref[1:2, :] == named)
    earlier = (iota((tokens, tokens), 0) < iota((tokens, tokens), 1)).astype(f32).astype(bf16)
    rank = dot(member.astype(f32).astype(bf16), earlier)
    code = jnp.where(member, rank, -1.0).astype(bf16)
    rows = experts * MAIN
    spread = (iota((rows, experts), 0) // MAIN == iota((rows, experts), 1)).astype(f32).astype(bf16)
    slot = (iota((rows, tokens), 0) % MAIN).astype(f32)
    chosen = (dot(spread, code) == slot).astype(f32).astype(bf16)
    main = dot(chosen, normed).astype(bf16)
    tiles = quarter // LANES
    for tile in range(tiles):
        out_ref[:, tile * MAIN : (tile + 1) * MAIN, :] = main[
            :, tile * LANES : (tile + 1) * LANES
        ].reshape(experts, MAIN, LANES)
    rest = 2 * tiles
    rows = experts * rest
    spread = (iota((rows, experts), 0) // rest == iota((rows, experts), 1)).astype(f32).astype(bf16)
    expanded = dot(spread, code)
    place = iota((rows, tokens), 0)
    hit = expanded == (MAIN + place % 2).astype(f32)
    summed = jnp.zeros((rows, LANES), f32)
    for tile in range(tiles):
        chosen = (hit & ((place % rest) // 2 == tile)).astype(f32).astype(bf16)
        summed = summed + dot(chosen, normed[:, tile * LANES : (tile + 1) * LANES])
    out_ref[:, tiles * MAIN :, :] = summed.reshape(experts, rest, LANES).astype(bf16)


def rest_order(sources, tiles, flip):
    size = sources * tiles * 2
    outer, inner = iota((size, size), 0), iota((size, size), 1)
    if flip:
        outer, inner = inner, outer
    tile, source, slot = outer // (2 * sources), (outer % (2 * sources)) // 2, outer % 2
    return (inner == source * 2 * tiles + tile * 2 + slot).astype(f32).astype(bf16)


def gathered_rows(x_ref, groups, sources):
    tiles = 4
    quarter = tiles * LANES
    half = sources // 2
    main_rows = sources * MAIN
    rests = []
    for index, pair in enumerate(groups):
        rest = []
        for side, (ref, first) in enumerate(pair):
            rows = half * MAIN
            for tile in range(tiles):
                block = ref[first : first + half, tile * MAIN : (tile + 1) * MAIN, :]
                lower = index * quarter + tile * LANES
                x_ref[side * rows : (side + 1) * rows, lower : lower + LANES] = block.reshape(
                    rows, LANES
                )
            rest.append(ref[first : first + half, tiles * MAIN :, :].astype(f32))
        rests.append(
            jnp.concatenate(rest, axis=0).reshape(sources * 2 * tiles, LANES).astype(bf16)
        )
    moved = dot(rest_order(sources, tiles, False), jnp.concatenate(rests, axis=1)).astype(bf16)
    for index in range(len(groups)):
        for tile in range(tiles):
            lower = index * quarter + tile * LANES
            x_ref[main_rows:, lower : lower + LANES] = moved[
                tile * 2 * sources : (tile + 1) * 2 * sources,
                index * LANES : (index + 1) * LANES,
            ]


def near_kernel(shifts, *refs):
    count = len(shifts)
    part_ref = refs[0]
    groups, place = [], 1
    for shift in shifts:
        if shift == 0:
            groups.append(((refs[place], 0), (refs[place], refs[place].shape[0] // 2)))
            place += 1
        else:
            groups.append(((refs[place], 0), (refs[place + 1], 0)))
            place += 2
    earlier_ref = None
    if shifts[0] != 0:
        earlier_ref = refs[place]
        place += 1
    g0_ref, u0_ref, g1_hbm, u1_hbm, sum_ref, x_ref, g1_ref, u1_ref, sems = refs[place:]
    quarter = 4 * LANES
    part = part_ref[0]
    starts = [pl.multiple_of(((part + shift) % 4) * quarter, quarter) for shift in shifts]
    copies = []
    for side, (source, target) in enumerate(((g1_hbm, g1_ref), (u1_hbm, u1_ref))):
        for index, start in enumerate(starts):
            copies.append(
                pltpu.make_async_copy(
                    source.at[pl.ds(start, quarter)],
                    target.at[pl.ds(index * quarter, quarter)],
                    sems.at[side * count + index],
                )
            )
    for copy in copies:
        copy.start()
    gathered_rows(x_ref, groups, x_ref.shape[0] // 18)
    for index in range(4):
        if index >= 2:
            for copy in copies[(index - 2) * count : (index - 1) * count]:
                copy.wait()
        total = None if earlier_ref is None else earlier_ref[index]
        for at, start in enumerate(starts):
            if index < 2:
                rows = (g0_ref, u0_ref)[index][pl.ds(start, quarter), :]
            else:
                rows = (g1_ref, u1_ref)[index - 2][at * quarter : (at + 1) * quarter, :]
            term = dot(x_ref[:, at * quarter : (at + 1) * quarter], rows)
            total = term if total is None else total + term
        sum_ref[index] = total


def far_kernel(
    part_ref, oa_ref, ob_ref, sum_ref, g0_ref, u0_ref, g1_hbm, u1_hbm, d0_ref, d1_hbm,
    own_out, ra_out, rb_out, la_out, lb_out, oa_out, ob_out,
    x_ref, hidden_ref, g1_ref, u1_ref, d1_ref, sems,
):
    half = oa_ref.shape[0]
    sources = 2 * half
    tiles = 4
    quarter = tiles * LANES
    units = g0_ref.shape[1]
    main_rows = sources * MAIN
    part = part_ref[0]
    starts = [pl.multiple_of(((part + shift) % 4) * quarter, quarter) for shift in (2, 3, 1, 0)]
    far = pl.ds(starts[0], quarter)
    copies = [
        pltpu.make_async_copy(g1_hbm.at[far], g1_ref, sems.at[0]),
        pltpu.make_async_copy(u1_hbm.at[far], u1_ref, sems.at[1]),
        pltpu.make_async_copy(d1_hbm, d1_ref, sems.at[2]),
    ]
    for copy in copies:
        copy.start()
    gathered_rows(x_ref, (((oa_ref, 0), (ob_ref, 0)),), sources)
    x = x_ref[...]
    for side in range(2):
        if side == 0:
            gate_rows, up_rows = g0_ref[far, :], u0_ref[far, :]
        else:
            copies[0].wait()
            copies[1].wait()
            gate_rows, up_rows = g1_ref[...], u1_ref[...]
        gate = sum_ref[2 * side] + dot(x, gate_rows)
        up = sum_ref[2 * side + 1] + dot(x, up_rows)
        hidden_ref[:, side * units : (side + 1) * units] = (
            gate / (1.0 + jnp.exp(-gate)) * up
        ).astype(bf16)
    copies[2].wait()
    targets = (
        ((oa_out, 0), (ob_out, 0)),
        ((la_out, 0), (lb_out, 0)),
        ((ra_out, 0), (rb_out, 0)),
        ((own_out, 0), (own_out, half)),
    )
    rests = []
    for start, pair in zip(starts, targets):
        result = (
            dot(hidden_ref[:, :units], d0_ref[:, pl.ds(start, quarter)])
            + dot(hidden_ref[:, units:], d1_ref[:, pl.ds(start, quarter)])
        ).astype(bf16)
        rows = half * MAIN
        for side, (ref, first) in enumerate(pair):
            for tile in range(tiles):
                ref[first : first + half, tile * MAIN : (tile + 1) * MAIN, :] = result[
                    side * rows : (side + 1) * rows, tile * LANES : (tile + 1) * LANES
                ].reshape(half, MAIN, LANES)
        rests.append(
            jnp.concatenate(
                [result[main_rows:, tile * LANES : (tile + 1) * LANES] for tile in range(tiles)],
                axis=0,
            )
        )
    moved = dot(rest_order(sources, tiles, True), jnp.concatenate(rests, axis=1))
    for index, pair in enumerate(targets):
        block = moved[:, index * LANES : (index + 1) * LANES].reshape(sources, 2 * tiles, LANES)
        for side, (ref, first) in enumerate(pair):
            ref[first : first + half, tiles * MAIN :, :] = block[
                side * half : (side + 1) * half
            ].astype(bf16)


def tail_kernel(
    back_ref, ids_ref, logits_ref, t0_ref, t1_ref, t2_ref, t3_ref, first_ref, out_ref
):
    first_ref[...] = (
        (t0_ref[...].astype(f32) + t1_ref[...].astype(f32))
        + (t2_ref[...].astype(f32) + t3_ref[...].astype(f32))
    ).astype(bf16)
    logits = logits_ref[...]
    shares = jax.nn.sigmoid(logits - jnp.concatenate([logits[1:2], logits[0:1]], axis=0))
    rows = jnp.concatenate(
        [ids_ref[...].astype(f32), shares, jnp.zeros((4, logits.shape[1]), f32)], axis=0
    )
    columns = jnp.transpose(rows)
    tokens, quarter = out_ref.shape
    experts = back_ref.shape[0]
    tiles = quarter // LANES
    rest = 2 * tiles
    named = iota((tokens, experts), 1)
    members = [columns[:, k : k + 1] == named.astype(f32) for k in range(2)]
    earlier = (iota((tokens, tokens), 1) < iota((tokens, tokens), 0)).astype(f32).astype(bf16)
    rank = dot(earlier, (members[0] | members[1]).astype(f32).astype(bf16))
    rows = experts * MAIN
    spread_main = (
        (iota((experts, rows), 1) // MAIN == iota((experts, rows), 0)).astype(f32).astype(bf16)
    )
    slot_main = (iota((tokens, rows), 1) % MAIN).astype(f32)
    rest_rows = experts * rest
    spread_rest = (
        (iota((experts, rest_rows), 1) // rest == iota((experts, rest_rows), 0))
        .astype(f32)
        .astype(bf16)
    )
    place = iota((tokens, rest_rows), 1)
    slot_rest = (MAIN + place % 2).astype(f32)
    main = jnp.concatenate(
        [
            back_ref[:, tile * MAIN : (tile + 1) * MAIN, :].reshape(rows, LANES)
            for tile in range(tiles)
        ],
        axis=1,
    )
    last = back_ref[:, tiles * MAIN :, :].astype(f32).reshape(rest_rows, LANES).astype(bf16)
    total = jnp.zeros((tokens, quarter), f32)
    for k in range(2):
        code = jnp.where(members[k], rank, -1.0).astype(bf16)
        chosen = (dot(code, spread_main) == slot_main).astype(f32).astype(bf16)
        picked = dot(chosen, main)
        hit = dot(code, spread_rest) == slot_rest
        extra = jnp.concatenate(
            [
                dot((hit & ((place % rest) // 2 == tile)).astype(f32).astype(bf16), last)
                for tile in range(tiles)
            ],
            axis=1,
        )
        total = total + columns[:, 2 + k : 3 + k] * (picked + extra)
    out_ref[...] = total.astype(bf16)


def pool_in_kernel(x_ref, gain_ref, inward_ref, pooled_ref, last_ref):
    rows, width = x_ref.shape
    block = 128
    for lower in range(0, rows, block):
        values = x_ref[lower : lower + block, :].astype(f32)
        mean = jnp.sum(values * values, axis=1, keepdims=True) / width
        normed = (values * lax.rsqrt(mean + epsilon) * gain_ref[...].astype(f32)).astype(bf16)
        pooled_ref[lower : lower + block, :] = dot(normed, inward_ref[...]).astype(bf16)
    last_ref[...] = pooled_ref[rows - HALO :, :]


def windows_kernel(
    part_ref, first_ref, pooled_ref, halo_ref, mixing_ref, scale_ref, outward_ref, *out_refs
):
    rows = pooled_ref.shape[0]
    part = part_ref[0]
    own = pooled_ref[...].astype(f32)
    total = jnp.concatenate([halo_ref[...].astype(f32), own], axis=0)
    chosen = None
    for level in range(4):
        total = total + pltpu.roll(total, 1 << level, 0)
        chosen = total if chosen is None else jnp.where(part >= level, total, chosen)
    window = jnp.left_shift(jnp.int32(2), part)
    positions = first_ref[0] + iota((rows, 1), 0)
    counts = jnp.minimum(positions + 1, window).astype(f32)
    mixed = (chosen[HALO:] / counts - own).astype(bf16)
    pooled = (dot(mixed, mixing_ref[0]) * scale_ref[...].astype(f32)).astype(bf16)
    for shift, ref in enumerate(out_refs):
        width = ref.shape[1]
        start = pl.multiple_of(((part + shift) % 4) * width, width)
        ref[...] = dot(pooled, outward_ref[:, pl.ds(start, width)]).astype(bf16)


VMEM = pl.BlockSpec(memory_space=pltpu.VMEM)
ANY = pl.BlockSpec(memory_space=pl.ANY)
SMEM = pl.BlockSpec(memory_space=pltpu.SMEM)
LARGE = pltpu.CompilerParams(vmem_limit_bytes=14 * 1024 * 1024)
SMALL = pltpu.CompilerParams(vmem_limit_bytes=12 * 1024 * 1024)


def both_halves(
    first_input,
    first_gain,
    pool_inward,
    pool_mixing,
    pool_scale,
    pool_outward,
    second_input,
    second_gain,
    route_ids,
    route_logits,
    expert_gate,
    expert_up,
    expert_down,
):
    experts = lax.axis_size("z") * lax.axis_size("y")
    width = first_input.shape[1]
    quarter = width // 4
    units = expert_gate.shape[2]
    tokens = second_input.shape[0]
    part = lax.axis_index("tp")
    part_array = part.reshape(1)
    message = jax.ShapeDtypeStruct((experts, 72, LANES), bf16)
    half_message = jax.ShapeDtypeStruct((experts // 2, 72, LANES), bf16)
    half = experts // 2

    swap = [(0, 1), (1, 0)]
    sent = pl.pallas_call(
        head_kernel,
        out_shape=message,
        in_specs=[SMEM, VMEM, VMEM, VMEM],
        out_specs=VMEM,
        compiler_params=SMALL,
        name="dispatch_rows",
    )(part_array, second_input, second_gain.reshape(1, width), route_ids.T)
    arrived = lax.all_to_all(sent, ZY, split_axis=0, concat_axis=0, tiled=True)
    gate_other = lax.ppermute(expert_gate[0], "core", swap)
    up_other = lax.ppermute(expert_up[0], "core", swap)
    down_other = lax.ppermute(expert_down[0], "core", swap)

    channels = jax.ShapeDtypeStruct((first_input.shape[0], pool_inward.shape[1]), bf16)
    pooled_in, last_rows = pl.pallas_call(
        pool_in_kernel,
        out_shape=(channels, jax.ShapeDtypeStruct((HALO, channels.shape[1]), bf16)),
        in_specs=[VMEM] * 3,
        out_specs=(VMEM,) * 2,
        compiler_params=SMALL,
        cost_estimate=pl.CostEstimate(flops=1 << 30, bytes_accessed=5 << 20, transcendentals=0),
        name="pool_in",
    )(first_input, first_gain.reshape(1, width), pool_inward)
    halo_rows = from_behind(last_rows, EP, 1)
    term = jax.ShapeDtypeStruct((first_input.shape[0], quarter), bf16)
    terms = pl.pallas_call(
        windows_kernel,
        out_shape=(term,) * 4,
        in_specs=[SMEM] * 2 + [VMEM] * 5,
        out_specs=(VMEM,) * 4,
        compiler_params=SMALL,
        cost_estimate=pl.CostEstimate(flops=1 << 29, bytes_accessed=3 << 20, transcendentals=0),
        name="windows",
    )(
        part_array,
        (lax.axis_index(EP) * first_input.shape[0]).reshape(1),
        pooled_in,
        halo_rows,
        pool_mixing,
        pool_scale.reshape(1, -1),
        pool_outward,
    )

    arrived, terms = lax.optimization_barrier((arrived, terms))
    first, second = arrived[:half], arrived[half:]
    left_a = shifted(first, "tp", 1)
    right_b = shifted(second, "tp", -1)
    left_b = shifted(second, "tp", 1)
    right_a = shifted(first, "tp", -1)
    over_a = shifted(left_a, "tp", 1)
    over_b = shifted(right_b, "tp", -1)
    term_far = shifted(terms[2], "tp", 2)

    gates = (expert_gate[0], expert_up[0], gate_other, up_other)
    products = experts * 18 * units * width
    sum_shape = jax.ShapeDtypeStruct((4, experts * 18, units), f32)

    def near(shifts, messages, earlier):
        count = len(shifts)
        return pl.pallas_call(
            functools.partial(near_kernel, shifts),
            out_shape=sum_shape,
            in_specs=[SMEM] + [VMEM] * (len(messages) + len(earlier) + 2) + [ANY] * 2,
            out_specs=VMEM,
            scratch_shapes=[
                pltpu.VMEM((experts * 18, count * quarter), bf16),
                pltpu.VMEM((count * quarter, units), bf16),
                pltpu.VMEM((count * quarter, units), bf16),
                pltpu.SemaphoreType.DMA((2 * count,)),
            ],
            compiler_params=LARGE,
            cost_estimate=pl.CostEstimate(
                flops=2 * count * products, bytes_accessed=4 << 20, transcendentals=0
            ),
        )(part_array, *messages, *earlier, *gates)

    sums = near((0,), (arrived,), ())
    sums = near((3, 1), (left_a, left_b, right_a, right_b), (sums,))
    outs = pl.pallas_call(
        far_kernel,
        out_shape=(message,) + (half_message,) * 6,
        in_specs=[SMEM] + [VMEM] * 5 + [ANY] * 2 + [VMEM, ANY],
        out_specs=(VMEM,) * 7,
        scratch_shapes=[
            pltpu.VMEM((experts * 18, quarter), bf16),
            pltpu.VMEM((experts * 18, 2 * units), bf16),
            pltpu.VMEM((quarter, units), bf16),
            pltpu.VMEM((quarter, units), bf16),
            pltpu.VMEM((units, width), bf16),
            pltpu.SemaphoreType.DMA((3,)),
        ],
        compiler_params=LARGE,
        cost_estimate=pl.CostEstimate(
            flops=6 * products, bytes_accessed=12 << 20, transcendentals=0
        ),
        name="far_quarter",
    )(part_array, over_a, over_b, sums, *gates, expert_down[0], down_other)
    own, to_right_a, to_right_b, to_left_a, to_left_b, to_over_a, to_over_b = outs

    passing_a = shifted(to_over_a, "tp", 1)
    passing_b = shifted(to_over_b, "tp", -1)
    from_left_b = shifted(to_right_b, "tp", 1)
    from_right_a = shifted(to_left_a, "tp", -1)
    from_left_a = shifted((to_right_a.astype(f32) + passing_a.astype(f32)).astype(bf16), "tp", 1)
    from_right_b = shifted((to_left_b.astype(f32) + passing_b.astype(f32)).astype(bf16), "tp", -1)
    term_left = shifted(terms[1], "tp", 1)
    term_right = shifted(terms[3], "tp", -1)
    summed = jnp.concatenate(
        [
            own[:half].astype(f32) + from_left_a.astype(f32) + from_right_a.astype(f32),
            own[half:].astype(f32) + from_left_b.astype(f32) + from_right_b.astype(f32),
        ],
        axis=0,
    ).astype(bf16)

    back = lax.all_to_all(summed, ZY, split_axis=0, concat_axis=0, tiled=True)

    back, term_far, term_left, term_right = lax.optimization_barrier(
        (back, term_far, term_left, term_right)
    )
    return pl.pallas_call(
        tail_kernel,
        out_shape=(term, jax.ShapeDtypeStruct((tokens, quarter), bf16)),
        in_specs=[VMEM] * 7,
        out_specs=(VMEM,) * 2,
        compiler_params=SMALL,
        name="combine_rows",
    )(back, route_ids.T, route_logits.T, terms[0], term_left, term_far, term_right)


def solution(mesh):
    split_mesh = Mesh(mesh.devices.reshape(8, 4, 2, 4), ("z", "y", "core", "tp"))
    placed = (
        P(EP, None),
        P(),
        P(None, "tp"),
        P("tp", None, None),
        P("tp"),
        P("tp", None),
        P(EP, None),
        P(),
        P(EP, None),
        P(EP, None),
        P(EP, None, "tp"),
        P(EP, None, "tp"),
        P(EP, "tp", None),
    )
    return jax.shard_map(
        both_halves,
        mesh=split_mesh,
        in_specs=placed,
        out_specs=(P(EP, "tp"), P(EP, "tp")),
        check_vma=False,
    )
```

profile of v0, /device:TPU:1, one launch (start us, length us, event | category | flops | bytes accessed | tf_op | source)
XLA Modules:
  0.0 130.0 jit_solution(2109843237153437489)
XLA Ops:
  0.6 3.3 %collective-permute-start.7 = (bf16[2048,512]{1,0:T(8,128)(2,1)}, bf16[2048,512]{1,0:T(8,128)(2,1)}, u32[]{:S(2)}, u32[]{:S(2)}) collective-permute-start(bf16[2048,512]{1,0:T(8,128)(2,1)} %bitcast.7), channel_id=1, source_target_pairs={{0,4},{4,0},{1,5},{5,1},{2,6},{6,2},{3,7},{7,3},{8,12},{12,8},{9,1... | collective-permute-start | bytes 6291464 | tf_op jit(solution)/shard_map/ppermute | solution.py:369
  6.6 1.7 %dispatch_rows.1 = bf16[32,72,128]{2,1,0:T(8,128)(2,1)} custom-call(s32[1]{0:T(128)} %bitcast.part_ref.refs_0_, bf16[256,2048]{1,0:T(8,128)(2,1)S(1)} %copy-done.2, bf16[1,2048]{1,0:T(2,128)(2,1)S(1)} %reshape.20.gain_ref, s32[2,256]{1,0:T(2,128)S(1)} %bitcast.15), custom_call_target="tpu_custom_call" | custom-call | tf_op jit(solution)/shard_map/dispatch_rows/pallas_call | solution.py:360
  8.3 9.6 %all-to-all-start = ((bf16[32,72,128]{2,1,0:T(8,128)(2,1)}), bf16[32,72,128]{2,1,0:T(8,128)(2,1)S(1)}, u32[]{:S(2)}, u32[]{:S(2)}) async-start(bf16[32,72,128]{2,1,0:T(8,128)(2,1)} %dispatch_rows.1), calls=%async_computation | async-start | bytes 1179648 | tf_op jit(solution)/shard_map/all_to_all | solution.py:368
  21.9 3.5 %collective-permute-start = (bf16[16,256]{1,0:T(8,128)(2,1)S(1)}, bf16[16,256]{1,0:T(8,128)(2,1)S(1)}, u32[]{:S(2)}, u32[]{:S(2)}) collective-permute-start(bf16[16,256]{1,0:T(8,128)(2,1)S(1)} %get-tuple-element.25), channel_id=1, source_target_pairs={{0,4},{4,8},{8,12},{12,16},{16,20},{20,24},{24,28},{28,32},{32,36}... | collective-permute-start | bytes 24584 | tf_op jit(solution)/shard_map/ppermute | solution.py:28
  28.3 1.7 %windows.1 = (bf16[512,512]{1,0:T(8,128)(2,1)S(1)}, bf16[512,512]{1,0:T(8,128)(2,1)}, bf16[512,512]{1,0:T(8,128)(2,1)}, bf16[512,512]{1,0:T(8,128)(2,1)S(1)}) custom-call(s32[1]{0:T(128)} %bitcast.part_ref.refs_0_, s32[1]{0:T(128)} %bitcast.2.first_ref, bf16[512,256]{1,0:T(8,128)(2,1)S(1)} %copy-done.13, bf16[16,256]{1,0:T(8,128)(2,1)S(1)} %collective-permute-done.halo_ref, ...), custom_call_target="tpu_custom_call" | custom-call | flops 536870912 | bytes 3145728 | tf_op jit(solution)/shard_map/windows/pallas_call | solution.py:385
  30.9 4.7 %all-to-all-done.refs_1_ = bf16[32,72,128]{2,1,0:T(8,128)(2,1)S(1)} async-done(((bf16[32,72,128]{2,1,0:T(8,128)(2,1)}), bf16[32,72,128]{2,1,0:T(8,128)(2,1)S(1)}, u32[]{:S(2)}, u32[]{:S(2)}) %all-to-all-start) | async-done | bytes 589856 | tf_op jit(solution)/shard_map/all_to_all | solution.py:368
  38.4 4.7 %collective-permute-done.1.refs_1_ = bf16[16,72,128]{2,1,0:T(8,128)(2,1)S(1)} collective-permute-done((bf16[16,72,128]{2,1,0:T(8,128)(2,1)S(1)}, bf16[16,72,128]{2,1,0:T(8,128)(2,1)S(1)}, u32[]{:S(2)}, u32[]{:S(2)}) %collective-permute-start.1) | collective-permute-done | bytes 294944 | tf_op jit(solution)/shard_map/ppermute | solution.py:22
  43.1 2.7 %collective-permute-start.6 = (bf16[16,72,128]{2,1,0:T(8,128)(2,1)S(1)}, bf16[16,72,128]{2,1,0:T(8,128)(2,1)S(1)}, u32[]{:S(2)}, u32[]{:S(2)}) collective-permute-start(bf16[16,72,128]{2,1,0:T(8,128)(2,1)S(1)} %get-tuple-element.49), channel_id=1, source_target_pairs={{0,3},{1,0},{2,1},{3,2},{4,7},{5,4},{6,5},{7,6},{8,11},{9,8},{10,9... | collective-permute-start | bytes 884744 | tf_op jit(solution)/shard_map/ppermute | solution.py:22
  45.7 2.7 %collective-permute-start.4 = (bf16[16,72,128]{2,1,0:T(8,128)(2,1)S(1)}, bf16[16,72,128]{2,1,0:T(8,128)(2,1)S(1)}, u32[]{:S(2)}, u32[]{:S(2)}) collective-permute-start(bf16[16,72,128]{2,1,0:T(8,128)(2,1)S(1)} %collective-permute-done.3.refs_4_), channel_id=1, source_target_pairs={{0,3},{1,0},{2,1},{3,2},{4,7},{5,4},{6,5},{7,6},{8,11},{9,8},{10,9... | collective-permute-start | bytes 884744 | tf_op jit(solution)/shard_map/ppermute | solution.py:22
  48.4 1.6 %copy-done.1 = bf16[1,2048,512]{2,1,0:T(8,128)(2,1)S(1)} copy-done((bf16[1,2048,512]{2,1,0:T(8,128)(2,1)S(1)}, bf16[1,2048,512]{2,1,0:T(8,128)(2,1)}, u32[]{:S(2)}) %copy-start.1) | copy-done | bytes 2097176
  50.0 2.4 %shard_map.140.refs_5_ = f32[4,576,512]{2,1,0:T(8,128)S(1)} custom-call(s32[1]{0:T(128)} %bitcast.part_ref.refs_0_, bf16[32,72,128]{2,1,0:T(8,128)(2,1)S(1)} %all-to-all-done.refs_1_, bf16[2048,512]{1,0:T(8,128)(2,1)S(1)} %bitcast.8, bf16[2048,512]{1,0:T(8,128)(2,1)S(1)} %bitcast.12, bf16[2048,512]{1,0:T(8,128)(2,1)} %collective-permute-done.7.refs_4_.refs_8_.g1_hbm, ...), custom_call_target="tpu_custom_call" | custom-call | flops 1207959552 | bytes 4194304 | tf_op jit(solution)/shard_map/pallas_call | solution.py:419
  52.5 3.1 %shard_map.141.sum_ref = f32[4,576,512]{2,1,0:T(8,128)S(1)} custom-call(s32[1]{0:T(128)} %bitcast.part_ref.refs_0_, bf16[16,72,128]{2,1,0:T(8,128)(2,1)S(1)} %collective-permute-done.1.refs_1_, bf16[16,72,128]{2,1,0:T(8,128)(2,1)S(1)} %collective-permute-done.5.refs_2_, bf16[16,72,128]{2,1,0:T(8,128)(2,1)S(1)} %collective-permute-done.6.refs_3_, ...), custom_call_target="tpu_custom_call" | custom-call | flops 2415919104 | bytes 4194304 | tf_op jit(solution)/shard_map/pallas_call | solution.py:419
  55.9 7.1 %far_quarter.1 = (bf16[32,72,128]{2,1,0:T(8,128)(2,1)S(1)}, bf16[16,72,128]{2,1,0:T(8,128)(2,1)S(1)}, bf16[16,72,128]{2,1,0:T(8,128)(2,1)S(1)}, bf16[16,72,128]{...) custom-call(s32[1]{0:T(128)} %bitcast.part_ref.refs_0_, ...), custom_call_target="tpu_custom_call" | custom-call | flops 3623878656 | bytes 12582912 | tf_op jit(solution)/shard_map/far_quarter/pallas_call | solution.py:438
  62.9 2.5 %collective-permute-start.14 = (bf16[16,72,128]{2,1,0:T(8,128)(2,1)S(1)}, bf16[16,72,128]{2,1,0:T(8,128)(2,1)S(1)}, u32[]{:S(2)}, u32[]{:S(2)}) collective-permute-start(bf16[16,72,128]{2,1,0:T(8,128)(2,1)S(1)} %get-tuple-element.37), channel_id=1, source_target_pairs={{0,3},{1,0},{2,1},{3,2},{4,7},{5,4},{6,5},{7,6},{8,11},{9,8},{10,9... | collective-permute-start | bytes 884744 | tf_op jit(solution)/shard_map/ppermute | solution.py:22
  65.4 2.7 %collective-permute-start.12 = (bf16[16,72,128]{2,1,0:T(8,128)(2,1)S(1)}, bf16[16,72,128]{2,1,0:T(8,128)(2,1)S(1)}, u32[]{:S(2)}, u32[]{:S(2)}) collective-permute-start(bf16[16,72,128]{2,1,0:T(8,128)(2,1)S(1)} %get-tuple-element.34), channel_id=1, source_target_pairs={{0,3},{1,0},{2,1},{3,2},{4,7},{5,4},{6,5},{7,6},{8,11},{9,8},{10,9... | collective-permute-start | bytes 884744 | tf_op jit(solution)/shard_map/ppermute | solution.py:22
  69.1 3.2 %collective-permute-start.15 = (bf16[16,72,128]{2,1,0:T(8,128)(2,1)S(1)}, bf16[16,72,128]{2,1,0:T(8,128)(2,1)S(1)}, u32[]{:S(2)}, u32[]{:S(2)}) collective-permute-start(bf16[16,72,128]{2,1,0:T(8,128)(2,1)S(1)} %add_convert_fusion.1), channel_id=1, source_target_pairs={{0,3},{1,0},{2,1},{3,2},{4,7},{5,4},{6,5},{7,6},{8,11},{9,8},{10,9... | collective-permute-start | bytes 884744 | tf_op jit(solution)/shard_map/ppermute | solution.py:22
  73.7 3.1 %collective-permute-done.13 = bf16[16,72,128]{2,1,0:T(8,128)(2,1)S(1)} collective-permute-done((bf16[16,72,128]{2,1,0:T(8,128)(2,1)S(1)}, bf16[16,72,128]{2,1,0:T(8,128)(2,1)S(1)}, u32[]{:S(2)}, u32[]{:S(2)}) %collective-permute-start.13) | collective-permute-done | bytes 294944 | tf_op jit(solution)/shard_map/ppermute | solution.py:22
  76.8 3.2 %collective-permute-done.15 = bf16[16,72,128]{2,1,0:T(8,128)(2,1)S(1)} collective-permute-done((bf16[16,72,128]{2,1,0:T(8,128)(2,1)S(1)}, bf16[16,72,128]{2,1,0:T(8,128)(2,1)S(1)}, u32[]{:S(2)}, u32[]{:S(2)}) %collective-permute-start.15) | collective-permute-done | bytes 294944 | tf_op jit(solution)/shard_map/ppermute | solution.py:22
  80.0 3.1 %collective-permute-done.11 = bf16[16,72,128]{2,1,0:T(8,128)(2,1)S(1)} collective-permute-done((bf16[16,72,128]{2,1,0:T(8,128)(2,1)S(1)}, bf16[16,72,128]{2,1,0:T(8,128)(2,1)S(1)}, u32[]{:S(2)}, u32[]{:S(2)}) %collective-permute-start.11) | collective-permute-done | bytes 294944 | tf_op jit(solution)/shard_map/ppermute | solution.py:22
  84.2 16.4 %all-to-all-start.1 = ((bf16[32,72,128]{2,1,0:T(8,128)(2,1)}), bf16[32,72,128]{2,1,0:T(8,128)(2,1)S(1)}, u32[]{:S(2)}, u32[]{:S(2)}) async-start(bf16[32,72,128]{2,1,0:T(8,128)(2,1)} %pad_maximum_fusion), calls=%async_computation.1 | async-start | bytes 1179648 | tf_op jit(solution)/shard_map/all_to_all | solution.py:475
  101.6 1.9 %collective-permute-start.18 = (bf16[512,512]{1,0:T(8,128)(2,1)S(1)}, bf16[512,512]{1,0:T(8,128)(2,1)S(1)}, u32[]{:S(2)}, u32[]{:S(2)}) collective-permute-start(bf16[512,512]{1,0:T(8,128)(2,1)S(1)} %copy-done.10), channel_id=1, source_target_pairs={{0,3},{1,0},{2,1},{3,2},{4,7},{5,4},{6,5},{7,6},{8,11},{9,8},{10,9... | collective-permute-start | bytes 1572872 | tf_op jit(solution)/shard_map/ppermute | solution.py:22
  103.5 10.9 %collective-permute-done.16.t2_ref = bf16[512,512]{1,0:T(8,128)(2,1)S(1)} collective-permute-done((bf16[512,512]{1,0:T(8,128)(2,1)}, bf16[512,512]{1,0:T(8,128)(2,1)S(1)}, u32[]{:S(2)}, u32[]{:S(2)}) %collective-permute-start.16) | collective-permute-done | bytes 524320 | tf_op jit(solution)/shard_map/ppermute | solution.py:22
  114.4 12.7 %collective-permute-done.17.t1_ref = bf16[512,512]{1,0:T(8,128)(2,1)S(1)} collective-permute-done((bf16[512,512]{1,0:T(8,128)(2,1)}, bf16[512,512]{1,0:T(8,128)(2,1)S(1)}, u32[]{:S(2)}, u32[]{:S(2)}) %collective-permute-start.17) | collective-permute-done | bytes 524320 | tf_op jit(solution)/shard_map/ppermute | solution.py:22
  127.1 2.8 %combine_rows.1 = (bf16[512,512]{1,0:T(8,128)(2,1)}, bf16[256,512]{1,0:T(8,128)(2,1)}) custom-call(bf16[32,72,128]{2,1,0:T(8,128)(2,1)S(1)} %all-to-all-done.1.back_ref, s32[2,256]{1,0:T(2,128)S(1)} %bitcast.16, f32[2,256]{1,0:T(2,128)S(1)} %bitcast.17, bf16[512,512]{1,0:T(8,128)(2,1)S(1)} %get-tuple-element.42.t0_ref, ...), custom_call_target="tpu_custom_call" | custom-call | tf_op jit(solution)/shard_map/combine_rows/pallas_call | solution.py:480
  (65 shorter events, 17.9 us)
Async XLA Ops:
  0.6 45.1 %collective-permute-start.7 = (bf16[2048,512]{1,0:T(8,128)(2,1)}, bf16[2048,512]{1,0:T(8,128)(2,1)}, u32[]{:S(2)}, u32[]{:S(2)}) collective-permute-start(bf16[2048,512]{1,0:T(8,128)(2,1)} %bitcast.7), channel_id=1, source_target_pairs={{0,4},{4,0},{1,5},{5,1},{2,6},{6,2},{3,7},{7,3},{8,12},{12,8},{9,1... | collective-permute-start | bytes 6291464 | tf_op jit(solution)/shard_map/ppermute | solution.py:369
  3.9 41.8 %collective-permute-start.8 = (bf16[2048,512]{1,0:T(8,128)(2,1)}, bf16[2048,512]{1,0:T(8,128)(2,1)}, u32[]{:S(2)}, u32[]{:S(2)}) collective-permute-start(bf16[2048,512]{1,0:T(8,128)(2,1)} %bitcast.11), channel_id=1, source_target_pairs={{0,4},{4,0},{1,5},{5,1},{2,6},{6,2},{3,7},{7,3},{8,12},{12,8},{9,1... | collective-permute-start | bytes 6291464 | tf_op jit(solution)/shard_map/ppermute | solution.py:370
  8.3 27.2 %all-to-all-start = ((bf16[32,72,128]{2,1,0:T(8,128)(2,1)}), bf16[32,72,128]{2,1,0:T(8,128)(2,1)S(1)}, u32[]{:S(2)}, u32[]{:S(2)}) async-start(bf16[32,72,128]{2,1,0:T(8,128)(2,1)} %dispatch_rows.1), calls=%async_computation | async-start | bytes 1179648 | tf_op jit(solution)/shard_map/all_to_all | solution.py:368
  18.0 37.9 %collective-permute-start.9 = (bf16[512,2048]{1,0:T(8,128)(2,1)}, bf16[512,2048]{1,0:T(8,128)(2,1)}, u32[]{:S(2)}, u32[]{:S(2)}) collective-permute-start(bf16[512,2048]{1,0:T(8,128)(2,1)} %bitcast.5.d0_ref), channel_id=1, source_target_pairs={{0,4},{4,0},{1,5},{5,1},{2,6},{6,2},{3,7},{7,3},{8,12},{12,8},{9,1... | collective-permute-start | bytes 6291464 | tf_op jit(solution)/shard_map/ppermute | solution.py:371
  21.9 26.5 %copy-start = (bf16[1,2048,512]{2,1,0:T(8,128)(2,1)S(1)}, bf16[1,2048,512]{2,1,0:T(8,128)(2,1)}, u32[]{:S(2)}) copy-start(bf16[1,2048,512]{2,1,0:T(8,128)(2,1)} %param.23) | copy-start | bytes 6291460
  21.9 4.2 %collective-permute-start = (bf16[16,256]{1,0:T(8,128)(2,1)S(1)}, bf16[16,256]{1,0:T(8,128)(2,1)S(1)}, u32[]{:S(2)}, u32[]{:S(2)}) collective-permute-start(bf16[16,256]{1,0:T(8,128)(2,1)S(1)} %get-tuple-element.25), channel_id=1, source_target_pairs={{0,4},{4,8},{8,12},{12,16},{16,20},{20,24},{24,28},{28,32},{32,36}... | collective-permute-start | bytes 24584 | tf_op jit(solution)/shard_map/ppermute | solution.py:28
  35.6 7.4 %collective-permute-start.1 = (bf16[16,72,128]{2,1,0:T(8,128)(2,1)S(1)}, bf16[16,72,128]{2,1,0:T(8,128)(2,1)S(1)}, u32[]{:S(2)}, u32[]{:S(2)}) collective-permute-start(bf16[16,72,128]{2,1,0:T(8,128)(2,1)S(1)} %get-tuple-element.49), channel_id=1, source_target_pairs={{0,1},{1,2},{2,3},{3,0},{4,5},{5,6},{6,7},{7,4},{8,9},{9,10},{10,1... | collective-permute-start | bytes 884744 | tf_op jit(solution)/shard_map/ppermute | solution.py:22
  36.9 6.1 %collective-permute-start.3 = (bf16[16,72,128]{2,1,0:T(8,128)(2,1)S(1)}, bf16[16,72,128]{2,1,0:T(8,128)(2,1)S(1)}, u32[]{:S(2)}, u32[]{:S(2)}) collective-permute-start(bf16[16,72,128]{2,1,0:T(8,128)(2,1)S(1)} %get-tuple-element.48), channel_id=1, source_target_pairs={{0,3},{1,0},{2,1},{3,2},{4,7},{5,4},{6,5},{7,6},{8,11},{9,8},{10,9... | collective-permute-start | bytes 884744 | tf_op jit(solution)/shard_map/ppermute | solution.py:22
  43.0 9.4 %collective-permute-start.5 = (bf16[16,72,128]{2,1,0:T(8,128)(2,1)S(1)}, bf16[16,72,128]{2,1,0:T(8,128)(2,1)S(1)}, u32[]{:S(2)}, u32[]{:S(2)}) collective-permute-start(bf16[16,72,128]{2,1,0:T(8,128)(2,1)S(1)} %get-tuple-element.48), channel_id=1, source_target_pairs={{0,1},{1,2},{2,3},{3,0},{4,5},{5,6},{6,7},{7,4},{8,9},{9,10},{10,1... | collective-permute-start | bytes 884744 | tf_op jit(solution)/shard_map/ppermute | solution.py:22
  43.1 9.4 %collective-permute-start.6 = (bf16[16,72,128]{2,1,0:T(8,128)(2,1)S(1)}, bf16[16,72,128]{2,1,0:T(8,128)(2,1)S(1)}, u32[]{:S(2)}, u32[]{:S(2)}) collective-permute-start(bf16[16,72,128]{2,1,0:T(8,128)(2,1)S(1)} %get-tuple-element.49), channel_id=1, source_target_pairs={{0,3},{1,0},{2,1},{3,2},{4,7},{5,4},{6,5},{7,6},{8,11},{9,8},{10,9... | collective-permute-start | bytes 884744 | tf_op jit(solution)/shard_map/ppermute | solution.py:22
  45.7 10.1 %collective-permute-start.2 = (bf16[16,72,128]{2,1,0:T(8,128)(2,1)S(1)}, bf16[16,72,128]{2,1,0:T(8,128)(2,1)S(1)}, u32[]{:S(2)}, u32[]{:S(2)}) collective-permute-start(bf16[16,72,128]{2,1,0:T(8,128)(2,1)S(1)} %collective-permute-done.1.refs_1_), channel_id=1, source_target_pairs={{0,1},{1,2},{2,3},{3,0},{4,5},{5,6},{6,7},{7,4},{8,9},{9,10},{10,1... | collective-permute-start | bytes 884744 | tf_op jit(solution)/shard_map/ppermute | solution.py:22
  45.7 10.1 %collective-permute-start.4 = (bf16[16,72,128]{2,1,0:T(8,128)(2,1)S(1)}, bf16[16,72,128]{2,1,0:T(8,128)(2,1)S(1)}, u32[]{:S(2)}, u32[]{:S(2)}) collective-permute-start(bf16[16,72,128]{2,1,0:T(8,128)(2,1)S(1)} %collective-permute-done.3.refs_4_), channel_id=1, source_target_pairs={{0,3},{1,0},{2,1},{3,2},{4,7},{5,4},{6,5},{7,6},{8,11},{9,8},{10,9... | collective-permute-start | bytes 884744 | tf_op jit(solution)/shard_map/ppermute | solution.py:22
  62.9 6.1 %collective-permute-start.14 = (bf16[16,72,128]{2,1,0:T(8,128)(2,1)S(1)}, bf16[16,72,128]{2,1,0:T(8,128)(2,1)S(1)}, u32[]{:S(2)}, u32[]{:S(2)}) collective-permute-start(bf16[16,72,128]{2,1,0:T(8,128)(2,1)S(1)} %get-tuple-element.37), channel_id=1, source_target_pairs={{0,3},{1,0},{2,1},{3,2},{4,7},{5,4},{6,5},{7,6},{8,11},{9,8},{10,9... | collective-permute-start | bytes 884744 | tf_op jit(solution)/shard_map/ppermute | solution.py:22
  65.4 6.9 %collective-permute-start.10 = (bf16[16,72,128]{2,1,0:T(8,128)(2,1)S(1)}, bf16[16,72,128]{2,1,0:T(8,128)(2,1)S(1)}, u32[]{:S(2)}, u32[]{:S(2)}) collective-permute-start(bf16[16,72,128]{2,1,0:T(8,128)(2,1)S(1)} %get-tuple-element.33), channel_id=1, source_target_pairs={{0,1},{1,2},{2,3},{3,0},{4,5},{5,6},{6,7},{7,4},{8,9},{9,10},{10,1... | collective-permute-start | bytes 884744 | tf_op jit(solution)/shard_map/ppermute | solution.py:22
  65.4 8.3 %collective-permute-start.12 = (bf16[16,72,128]{2,1,0:T(8,128)(2,1)S(1)}, bf16[16,72,128]{2,1,0:T(8,128)(2,1)S(1)}, u32[]{:S(2)}, u32[]{:S(2)}) collective-permute-start(bf16[16,72,128]{2,1,0:T(8,128)(2,1)S(1)} %get-tuple-element.34), channel_id=1, source_target_pairs={{0,3},{1,0},{2,1},{3,2},{4,7},{5,4},{6,5},{7,6},{8,11},{9,8},{10,9... | collective-permute-start | bytes 884744 | tf_op jit(solution)/shard_map/ppermute | solution.py:22
  68.1 8.7 %collective-permute-start.13 = (bf16[16,72,128]{2,1,0:T(8,128)(2,1)S(1)}, bf16[16,72,128]{2,1,0:T(8,128)(2,1)S(1)}, u32[]{:S(2)}, u32[]{:S(2)}) collective-permute-start(bf16[16,72,128]{2,1,0:T(8,128)(2,1)S(1)} %get-tuple-element.35), channel_id=1, source_target_pairs={{0,1},{1,2},{2,3},{3,0},{4,5},{5,6},{6,7},{7,4},{8,9},{9,10},{10,1... | collective-permute-start | bytes 884744 | tf_op jit(solution)/shard_map/ppermute | solution.py:22
  69.1 10.9 %collective-permute-start.15 = (bf16[16,72,128]{2,1,0:T(8,128)(2,1)S(1)}, bf16[16,72,128]{2,1,0:T(8,128)(2,1)S(1)}, u32[]{:S(2)}, u32[]{:S(2)}) collective-permute-start(bf16[16,72,128]{2,1,0:T(8,128)(2,1)S(1)} %add_convert_fusion.1), channel_id=1, source_target_pairs={{0,3},{1,0},{2,1},{3,2},{4,7},{5,4},{6,5},{7,6},{8,11},{9,8},{10,9... | collective-permute-start | bytes 884744 | tf_op jit(solution)/shard_map/ppermute | solution.py:22
  72.4 10.7 %collective-permute-start.11 = (bf16[16,72,128]{2,1,0:T(8,128)(2,1)S(1)}, bf16[16,72,128]{2,1,0:T(8,128)(2,1)S(1)}, u32[]{:S(2)}, u32[]{:S(2)}) collective-permute-start(bf16[16,72,128]{2,1,0:T(8,128)(2,1)S(1)} %add_convert_fusion.3), channel_id=1, source_target_pairs={{0,1},{1,2},{2,3},{3,0},{4,5},{5,6},{6,7},{7,4},{8,9},{9,10},{10,1... | collective-permute-start | bytes 884744 | tf_op jit(solution)/shard_map/ppermute | solution.py:22
  83.1 44.0 %copy-start.4 = (s32[256,2]{0,1:T(2,128)S(1)}, s32[256,2]{0,1:T(2,128)}, u32[]{:S(2)}) copy-start(s32[256,2]{0,1:T(2,128)} %param.21) | copy-start | bytes 6148
  83.1 44.0 %copy-start.5 = (f32[256,2]{0,1:T(2,128)S(1)}, f32[256,2]{0,1:T(2,128)}, u32[]{:S(2)}) copy-start(f32[256,2]{0,1:T(2,128)} %param.22) | copy-start | bytes 6148
  84.2 42.9 %all-to-all-start.1 = ((bf16[32,72,128]{2,1,0:T(8,128)(2,1)}), bf16[32,72,128]{2,1,0:T(8,128)(2,1)S(1)}, u32[]{:S(2)}, u32[]{:S(2)}) async-start(bf16[32,72,128]{2,1,0:T(8,128)(2,1)} %pad_maximum_fusion), calls=%async_computation.1 | async-start | bytes 1179648 | tf_op jit(solution)/shard_map/all_to_all | solution.py:475
  100.6 13.7 %collective-permute-start.16 = (bf16[512,512]{1,0:T(8,128)(2,1)}, bf16[512,512]{1,0:T(8,128)(2,1)S(1)}, u32[]{:S(2)}, u32[]{:S(2)}) collective-permute-start(bf16[512,512]{1,0:T(8,128)(2,1)} %get-tuple-element.38), channel_id=1, source_target_pairs={{0,2},{1,3},{2,0},{3,1},{4,6},{5,7},{6,4},{7,5},{8,10},{9,11},{10,... | collective-permute-start | bytes 1572872 | tf_op jit(solution)/shard_map/ppermute | solution.py:22
  100.7 26.4 %collective-permute-start.17 = (bf16[512,512]{1,0:T(8,128)(2,1)}, bf16[512,512]{1,0:T(8,128)(2,1)S(1)}, u32[]{:S(2)}, u32[]{:S(2)}) collective-permute-start(bf16[512,512]{1,0:T(8,128)(2,1)} %get-tuple-element.39), channel_id=1, source_target_pairs={{0,1},{1,2},{2,3},{3,0},{4,5},{5,6},{6,7},{7,4},{8,9},{9,10},{10,1... | collective-permute-start | bytes 1572872 | tf_op jit(solution)/shard_map/ppermute | solution.py:22
  101.6 25.5 %collective-permute-start.18 = (bf16[512,512]{1,0:T(8,128)(2,1)S(1)}, bf16[512,512]{1,0:T(8,128)(2,1)S(1)}, u32[]{:S(2)}, u32[]{:S(2)}) collective-permute-start(bf16[512,512]{1,0:T(8,128)(2,1)S(1)} %copy-done.10), channel_id=1, source_target_pairs={{0,3},{1,0},{2,1},{3,2},{4,7},{5,4},{6,5},{7,6},{8,11},{9,8},{10,9... | collective-permute-start | bytes 1572872 | tf_op jit(solution)/shard_map/ppermute | solution.py:22
  (13 other events, 82.4 us)
where the time goes:
time: 131 us; the launch traced here: 130 us
  starting transfers between devices  53 us (40%)
  waiting for transfers between devices  45.5 us (35%)
  Pallas kernels  20.1 us (15%)
  local copies, waits for them, and re-layouts  9.21 us (7%)
    ppermute x15, waiting for transfers between devices, shifted(): lax.ppermute(value, axis, [(i, (i + steps) % count) for i in range(count)])  40.1 us
    ppermute x15, starting transfers between devices, shifted(): lax.ppermute(value, axis, [(i, (i + steps) % count) for i in range(count)])  19.4 us
    all_to_all x1, starting transfers between devices, both_halves(): back = lax.all_to_all(summed, ZY, split_axis=0, concat_axis=0, tiled=True)  16.4 us
    all_to_all x1, starting transfers between devices, both_halves(): arrived = lax.all_to_all(sent, ZY, split_axis=0, concat_axis=0, tiled=True)  9.63 us
    unnamed x32, local copies, waits for them, and re-layouts  8.46 us
    pallas_call x1, Pallas kernels, both_halves(): pl.pallas_call(far_kernel, out_shape=(message,) + (half_message,) * 6, in...  7.07 us
    pallas_call x2, Pallas kernels, near(): pl.pallas_call(functools.partial(near_kernel, shifts), out_shape=sum_shap...  5.54 us
    all_to_all x1, waiting for transfers between devices, both_halves(): arrived = lax.all_to_all(sent, ZY, split_axis=0, concat_axis=0, tiled=True)  4.7 us
  transfers between devices with their start and end apart: 21, of which 11 were waited for; matrix products, arithmetic and copies ran while one was open for 1% of the time, Pallas kernels for 8%

commit v1 on v0

--- a/solution.py
+++ b/solution.py
@@ -47,7 +47,17 @@
     inverse = lax.rsqrt(total / width + epsilon)
     start = pl.multiple_of(part_ref[0] * quarter, quarter)
     mine = x_ref[:, pl.ds(start, quarter)].astype(f32)
-    normed = (mine * inverse * gain_ref[:, pl.ds(start, quarter)].astype(f32)).astype(bf16)
+    gains = gain_ref[...].astype(f32)
+    tile_rows = iota(gains.shape, 0)
+    first_tile = part_ref[0] * (quarter // LANES)
+    gain = jnp.concatenate(
+        [
+            jnp.sum(jnp.where(tile_rows == first_tile + tile, gains, 0.0), axis=0, keepdims=True)
+            for tile in range(quarter // LANES)
+        ],
+        axis=1,
+    )
+    normed = (mine * inverse * gain).astype(bf16)
     named = iota((experts, tokens), 0)
     member = (ids_ref[0:1, :] == named) | (ids_ref[1:2, :] == named)
     earlier = (iota((tokens, tokens), 0) < iota((tokens, tokens), 1)).astype(f32).astype(bf16)
@@ -164,15 +174,14 @@
 
 def far_kernel(
     part_ref, oa_ref, ob_ref, sum_ref, g0_ref, u0_ref, g1_hbm, u1_hbm, d0_ref, d1_hbm,
-    own_out, ra_out, rb_out, la_out, lb_out, oa_out, ob_out,
-    x_ref, hidden_ref, g1_ref, u1_ref, d1_ref, sems,
+    oa_out, ob_out, hidden_ref,
+    x_ref, g1_ref, u1_ref, d1_ref, sems,
 ):
     half = oa_ref.shape[0]
     sources = 2 * half
     tiles = 4
     quarter = tiles * LANES
     units = g0_ref.shape[1]
-    main_rows = sources * MAIN
     part = part_ref[0]
     starts = [pl.multiple_of(((part + shift) % 4) * quarter, quarter) for shift in (2, 3, 1, 0)]
     far = pl.ds(starts[0], quarter)
@@ -198,14 +207,18 @@
             gate / (1.0 + jnp.exp(-gate)) * up
         ).astype(bf16)
     copies[2].wait()
-    targets = (
-        ((oa_out, 0), (ob_out, 0)),
-        ((la_out, 0), (lb_out, 0)),
-        ((ra_out, 0), (rb_out, 0)),
-        ((own_out, 0), (own_out, half)),
-    )
+    down_terms(part, (2,), hidden_ref, d0_ref, d1_ref, (((oa_out, 0), (ob_out, 0)),), sources)
+
+
+def down_terms(part, shifts, hidden_ref, d0_ref, d1_ref, targets, sources):
+    tiles = 4
+    quarter = tiles * LANES
+    half = sources // 2
+    units = d0_ref.shape[0]
+    main_rows = sources * MAIN
     rests = []
-    for start, pair in zip(starts, targets):
+    for shift, pair in zip(shifts, targets):
+        start = pl.multiple_of(((part + shift) % 4) * quarter, quarter)
         result = (
             dot(hidden_ref[:, :units], d0_ref[:, pl.ds(start, quarter)])
             + dot(hidden_ref[:, units:], d1_ref[:, pl.ds(start, quarter)])
@@ -231,28 +244,35 @@
             ].astype(bf16)
 
 
-def tail_kernel(
-    back_ref, ids_ref, logits_ref, t0_ref, t1_ref, t2_ref, t3_ref, first_ref, out_ref
+def rest_kernel(
+    part_ref, hidden_ref, d0_ref, d1_ref, own_out, ra_out, rb_out, la_out, lb_out
 ):
-    first_ref[...] = (
-        (t0_ref[...].astype(f32) + t1_ref[...].astype(f32))
-        + (t2_ref[...].astype(f32) + t3_ref[...].astype(f32))
-    ).astype(bf16)
+    half = ra_out.shape[0]
+    targets = (
+        ((la_out, 0), (lb_out, 0)),
+        ((ra_out, 0), (rb_out, 0)),
+        ((own_out, 0), (own_out, half)),
+    )
+    down_terms(part_ref[0], (3, 1, 0), hidden_ref, d0_ref, d1_ref, targets, 2 * half)
+
+
+def prepare_kernel(ids_ref, logits_ref, main_ref, rest_ref, shares_ref):
+    tokens = ids_ref.shape[1]
+    rows = main_ref.shape[2]
+    experts = rows // MAIN
+    rest = rest_ref.shape[2] // experts
     logits = logits_ref[...]
     shares = jax.nn.sigmoid(logits - jnp.concatenate([logits[1:2], logits[0:1]], axis=0))
-    rows = jnp.concatenate(
-        [ids_ref[...].astype(f32), shares, jnp.zeros((4, logits.shape[1]), f32)], axis=0
-    )
-    columns = jnp.transpose(rows)
-    tokens, quarter = out_ref.shape
-    experts = back_ref.shape[0]
-    tiles = quarter // LANES
-    rest = 2 * tiles
-    named = iota((tokens, experts), 1)
-    members = [columns[:, k : k + 1] == named.astype(f32) for k in range(2)]
+    columns = jnp.transpose(
+        jnp.concatenate(
+            [shares, ids_ref[...].astype(f32), jnp.zeros((4, tokens), f32)], axis=0
+        )
+    )
+    shares_ref[...] = columns
+    named = iota((tokens, experts), 1).astype(f32)
+    members = [columns[:, 2 + k : 3 + k] == named for k in range(2)]
     earlier = (iota((tokens, tokens), 1) < iota((tokens, tokens), 0)).astype(f32).astype(bf16)
     rank = dot(earlier, (members[0] | members[1]).astype(f32).astype(bf16))
-    rows = experts * MAIN
     spread_main = (
         (iota((experts, rows), 1) // MAIN == iota((experts, rows), 0)).astype(f32).astype(bf16)
     )
@@ -265,6 +285,16 @@
     )
     place = iota((tokens, rest_rows), 1)
     slot_rest = (MAIN + place % 2).astype(f32)
+    for k in range(2):
+        code = jnp.where(members[k], rank, -1.0).astype(bf16)
+        main_ref[k] = (dot(code, spread_main) == slot_main).astype(f32).astype(bf16)
+        rest_ref[k] = (dot(code, spread_rest) == slot_rest).astype(f32).astype(bf16)
+
+
+def tail_kernel(back_ref, main_ref, rest_ref, shares_ref, out_ref):
+    experts = back_ref.shape[0]
+    tiles = out_ref.shape[1] // LANES
+    rows = experts * MAIN
     main = jnp.concatenate(
         [
             back_ref[:, tile * MAIN : (tile + 1) * MAIN, :].reshape(rows, LANES)
@@ -272,38 +302,33 @@
         ],
         axis=1,
     )
-    last = back_ref[:, tiles * MAIN :, :].astype(f32).reshape(rest_rows, LANES).astype(bf16)
-    total = jnp.zeros((tokens, quarter), f32)
+    last = back_ref[:, tiles * MAIN :, :].astype(f32).reshape(-1, LANES)
+    owner = (iota(last.shape, 0) % (2 * tiles)) // 2
+    last = jnp.concatenate(
+        [jnp.where(owner == tile, last, 0.0) for tile in range(tiles)], axis=1
+    ).astype(bf16)
+    total = None
     for k in range(2):
-        code = jnp.where(members[k], rank, -1.0).astype(bf16)
-        chosen = (dot(code, spread_main) == slot_main).astype(f32).astype(bf16)
-        picked = dot(chosen, main)
-        hit = dot(code, spread_rest) == slot_rest
-        extra = jnp.concatenate(
-            [
-                dot((hit & ((place % rest) // 2 == tile)).astype(f32).astype(bf16), last)
-                for tile in range(tiles)
-            ],
-            axis=1,
-        )
-        total = total + columns[:, 2 + k : 3 + k] * (picked + extra)
+        extra = dot(rest_ref[k], last)
+        term = shares_ref[:, k : k + 1] * (dot(main_ref[k], main) + extra)
+        total = term if total is None else total + term
     out_ref[...] = total.astype(bf16)
 
 
 def pool_in_kernel(x_ref, gain_ref, inward_ref, pooled_ref, last_ref):
     rows, width = x_ref.shape
     block = 128
+    gains = gain_ref[...].astype(f32)
+    gain = jnp.concatenate([gains[tile : tile + 1] for tile in range(width // LANES)], axis=1)
     for lower in range(0, rows, block):
         values = x_ref[lower : lower + block, :].astype(f32)
         mean = jnp.sum(values * values, axis=1, keepdims=True) / width
-        normed = (values * lax.rsqrt(mean + epsilon) * gain_ref[...].astype(f32)).astype(bf16)
+        normed = (values * lax.rsqrt(mean + epsilon) * gain).astype(bf16)
         pooled_ref[lower : lower + block, :] = dot(normed, inward_ref[...]).astype(bf16)
     last_ref[...] = pooled_ref[rows - HALO :, :]
 
 
-def windows_kernel(
-    part_ref, first_ref, pooled_ref, halo_ref, mixing_ref, scale_ref, outward_ref, *out_refs
-):
+def windows_kernel(part_ref, first_ref, pooled_ref, halo_ref, mixing_ref, scale_ref, out_ref):
     rows = pooled_ref.shape[0]
     part = part_ref[0]
     own = pooled_ref[...].astype(f32)
@@ -316,11 +341,23 @@
     positions = first_ref[0] + iota((rows, 1), 0)
     counts = jnp.minimum(positions + 1, window).astype(f32)
     mixed = (chosen[HALO:] / counts - own).astype(bf16)
-    pooled = (dot(mixed, mixing_ref[0]) * scale_ref[...].astype(f32)).astype(bf16)
-    for shift, ref in enumerate(out_refs):
-        width = ref.shape[1]
-        start = pl.multiple_of(((part + shift) % 4) * width, width)
-        ref[...] = dot(pooled, outward_ref[:, pl.ds(start, width)]).astype(bf16)
+    out_ref[...] = (dot(mixed, mixing_ref[0]) * scale_ref[...].astype(f32)).astype(bf16)
+
+
+def pool_out_kernel(*refs):
+    total = dot(refs[0][...], refs[4][...])
+    for channels, weights in zip(refs[1:4], refs[5:8]):
+        total = total + dot(channels[...], weights[...])
+    refs[8][...] = total.astype(bf16)
+
+
+def sum_kernel(own_ref, la_ref, ra_ref, lb_ref, rb_ref, out_ref):
+    half = la_ref.shape[0]
+    for first, refs in ((0, (la_ref, ra_ref)), (half, (lb_ref, rb_ref))):
+        total = own_ref[first : first + half].astype(f32)
+        out_ref[first : first + half] = (
+            total + refs[0][...].astype(f32) + refs[1][...].astype(f32)
+        ).astype(bf16)
 
 
 VMEM = pl.BlockSpec(memory_space=pltpu.VMEM)
@@ -364,7 +401,8 @@
         out_specs=VMEM,
         compiler_params=SMALL,
         name="dispatch_rows",
-    )(part_array, second_input, second_gain.reshape(1, width), route_ids.T)
+    )(part_array, second_input, second_gain.reshape(width // LANES, LANES), route_ids.T)
+    sent, pool_outward = lax.optimization_barrier((sent, pool_outward))
     arrived = lax.all_to_all(sent, ZY, split_axis=0, concat_axis=0, tiled=True)
     gate_other = lax.ppermute(expert_gate[0], "core", swap)
     up_other = lax.ppermute(expert_up[0], "core", swap)
@@ -379,28 +417,15 @@
         compiler_params=SMALL,
         cost_estimate=pl.CostEstimate(flops=1 << 30, bytes_accessed=5 << 20, transcendentals=0),
         name="pool_in",
-    )(first_input, first_gain.reshape(1, width), pool_inward)
+    )(first_input, first_gain.reshape(width // LANES, LANES), pool_inward)
     halo_rows = from_behind(last_rows, EP, 1)
-    term = jax.ShapeDtypeStruct((first_input.shape[0], quarter), bf16)
-    terms = pl.pallas_call(
-        windows_kernel,
-        out_shape=(term,) * 4,
-        in_specs=[SMEM] * 2 + [VMEM] * 5,
-        out_specs=(VMEM,) * 4,
-        compiler_params=SMALL,
-        cost_estimate=pl.CostEstimate(flops=1 << 29, bytes_accessed=3 << 20, transcendentals=0),
-        name="windows",
-    )(
-        part_array,
-        (lax.axis_index(EP) * first_input.shape[0]).reshape(1),
-        pooled_in,
-        halo_rows,
-        pool_mixing,
-        pool_scale.reshape(1, -1),
-        pool_outward,
-    )
-
-    arrived, terms = lax.optimization_barrier((arrived, terms))
+    slices = [
+        lax.dynamic_slice_in_dim(pool_outward, ((part + shift) % 4) * quarter, quarter, 1)
+        for shift in range(4)
+    ]
+    outward = [shifted(slices[shift], "tp", shift) for shift in (1, 2, 3)]
+
+    arrived, pooled_in = lax.optimization_barrier((arrived, pooled_in))
     first, second = arrived[:half], arrived[half:]
     left_a = shifted(first, "tp", 1)
     right_b = shifted(second, "tp", -1)
@@ -408,7 +433,6 @@
     right_a = shifted(first, "tp", -1)
     over_a = shifted(left_a, "tp", 1)
     over_b = shifted(right_b, "tp", -1)
-    term_far = shifted(terms[2], "tp", 2)
 
     gates = (expert_gate[0], expert_up[0], gate_other, up_other)
     products = experts * 18 * units * width
@@ -435,14 +459,14 @@
 
     sums = near((0,), (arrived,), ())
     sums = near((3, 1), (left_a, left_b, right_a, right_b), (sums,))
-    outs = pl.pallas_call(
+    to_over_a, to_over_b, hidden = pl.pallas_call(
         far_kernel,
-        out_shape=(message,) + (half_message,) * 6,
+        out_shape=(half_message,) * 2
+        + (jax.ShapeDtypeStruct((experts * 18, 2 * units), bf16),),
         in_specs=[SMEM] + [VMEM] * 5 + [ANY] * 2 + [VMEM, ANY],
-        out_specs=(VMEM,) * 7,
+        out_specs=(VMEM,) * 3,
         scratch_shapes=[
             pltpu.VMEM((experts * 18, quarter), bf16),
-            pltpu.VMEM((experts * 18, 2 * units), bf16),
             pltpu.VMEM((quarter, units), bf16),
             pltpu.VMEM((quarter, units), bf16),
             pltpu.VMEM((units, width), bf16),
@@ -450,41 +474,90 @@
         ],
         compiler_params=LARGE,
         cost_estimate=pl.CostEstimate(
-            flops=6 * products, bytes_accessed=12 << 20, transcendentals=0
+            flops=3 * products, bytes_accessed=12 << 20, transcendentals=0
         ),
         name="far_quarter",
     )(part_array, over_a, over_b, sums, *gates, expert_down[0], down_other)
-    own, to_right_a, to_right_b, to_left_a, to_left_b, to_over_a, to_over_b = outs
+    own, to_right_a, to_right_b, to_left_a, to_left_b = pl.pallas_call(
+        rest_kernel,
+        out_shape=(message,) + (half_message,) * 4,
+        in_specs=[SMEM] + [VMEM] * 3,
+        out_specs=(VMEM,) * 5,
+        compiler_params=LARGE,
+        cost_estimate=pl.CostEstimate(
+            flops=3 * products, bytes_accessed=8 << 20, transcendentals=0
+        ),
+        name="rest_terms",
+    )(part_array, hidden, expert_down[0], down_other)
 
     passing_a = shifted(to_over_a, "tp", 1)
     passing_b = shifted(to_over_b, "tp", -1)
     from_left_b = shifted(to_right_b, "tp", 1)
     from_right_a = shifted(to_left_a, "tp", -1)
+    pooled_in, halo_rows, passing_a, passing_b = lax.optimization_barrier(
+        (pooled_in, halo_rows, passing_a, passing_b)
+    )
     from_left_a = shifted((to_right_a.astype(f32) + passing_a.astype(f32)).astype(bf16), "tp", 1)
     from_right_b = shifted((to_left_b.astype(f32) + passing_b.astype(f32)).astype(bf16), "tp", -1)
-    term_left = shifted(terms[1], "tp", 1)
-    term_right = shifted(terms[3], "tp", -1)
-    summed = jnp.concatenate(
-        [
-            own[:half].astype(f32) + from_left_a.astype(f32) + from_right_a.astype(f32),
-            own[half:].astype(f32) + from_left_b.astype(f32) + from_right_b.astype(f32),
-        ],
-        axis=0,
-    ).astype(bf16)
-
+    pooled = pl.pallas_call(
+        windows_kernel,
+        out_shape=channels,
+        in_specs=[SMEM] * 2 + [VMEM] * 4,
+        out_specs=VMEM,
+        compiler_params=SMALL,
+        cost_estimate=pl.CostEstimate(flops=1 << 28, bytes_accessed=1 << 20, transcendentals=0),
+        name="windows",
+    )(
+        part_array,
+        (lax.axis_index(EP) * first_input.shape[0]).reshape(1),
+        pooled_in,
+        halo_rows,
+        pool_mixing,
+        pool_scale.reshape(1, -1),
+    )
+    summed = pl.pallas_call(
+        sum_kernel,
+        out_shape=message,
+        in_specs=[VMEM] * 5,
+        out_specs=VMEM,
+        compiler_params=SMALL,
+        name="ring_sum",
+    )(own, from_left_a, from_right_a, from_left_b, from_right_b)
+    summed, pooled = lax.optimization_barrier((summed, pooled))
     back = lax.all_to_all(summed, ZY, split_axis=0, concat_axis=0, tiled=True)
-
-    back, term_far, term_left, term_right = lax.optimization_barrier(
-        (back, term_far, term_left, term_right)
-    )
-    return pl.pallas_call(
+    pooled_far = shifted(pooled, "tp", 2)
+    pooled_sides = [shifted(pooled, "tp", shift) for shift in (1, 3)]
+    others = [pooled_sides[0], pooled_far, pooled_sides[1]]
+    first_out = pl.pallas_call(
+        pool_out_kernel,
+        out_shape=jax.ShapeDtypeStruct((first_input.shape[0], quarter), bf16),
+        in_specs=[VMEM] * 8,
+        out_specs=VMEM,
+        compiler_params=SMALL,
+        cost_estimate=pl.CostEstimate(flops=1 << 29, bytes_accessed=2 << 20, transcendentals=0),
+        name="pool_out",
+    )(pooled, *others, slices[0], *outward)
+    chosen_main, chosen_rest, shares = pl.pallas_call(
+        prepare_kernel,
+        out_shape=(
+            jax.ShapeDtypeStruct((2, tokens, experts * MAIN), bf16),
+            jax.ShapeDtypeStruct((2, tokens, experts * 8), bf16),
+            jax.ShapeDtypeStruct((tokens, 8), f32),
+        ),
+        in_specs=[VMEM] * 2,
+        out_specs=(VMEM,) * 3,
+        compiler_params=SMALL,
+        name="combine_prepare",
+    )(route_ids.T, route_logits.T)
+    second_out = pl.pallas_call(
         tail_kernel,
-        out_shape=(term, jax.ShapeDtypeStruct((tokens, quarter), bf16)),
-        in_specs=[VMEM] * 7,
-        out_specs=(VMEM,) * 2,
+        out_shape=jax.ShapeDtypeStruct((tokens, quarter), bf16),
+        in_specs=[VMEM] * 4,
+        out_specs=VMEM,
         compiler_params=SMALL,
         name="combine_rows",
-    )(back, route_ids.T, route_logits.T, terms[0], term_left, term_far, term_right)
+    )(back, chosen_main, chosen_rest, shares)
+    return (first_out, second_out)
 
 
 def solution(mesh):

time: 131 us -> 132 us (level)
  starting transfers between devices: 53 us -> 48.6 us
  waiting for transfers between devices: 45.5 us -> 49 us
  Pallas kernels: 20.1 us -> 23 us
    all_to_all x1, starting transfers between devices: 16.4 us -> 7.34 us  [both_halves(): back = lax.all_to_all(summed, ZY, split_axis=0, concat_axis=0, tiled=True)]
    all_to_all x1, waiting for transfers between devices: 4.7 us -> 12.9 us  [both_halves(): arrived = lax.all_to_all(sent, ZY, split_axis=0, concat_axis=0, tiled=True)]
    ppermute x15 -> x18, waiting for transfers between devices: 40.1 us -> 36.2 us  [shifted(): lax.ppermute(value, axis, [(i, (i + steps) % count) for i in range(count)])]
    ppermute x1, starting transfers between devices: 3.45 us -> 7.39 us  [from_behind(): lax.ppermute(value, axis, [(source, source + steps) for source in range(l...]
    pallas_call x3 -> x7, Pallas kernels: 11.6 us -> 14.6 us  [the longest x1 4.88 us: both_halves(): pl.pallas_call(far_kernel, out_shape=(half_message,) * 2 + (jax.ShapeDtyp...]
    unnamed x32 -> x24, local copies, waits for them, and re-layouts: 8.46 us -> 7.03 us
    ppermute x15 -> x18, starting transfers between devices: 19.4 us -> 20.3 us  [shifted(): lax.ppermute(value, axis, [(i, (i + steps) % count) for i in range(count)])]
  transfers between devices with their start and end apart: 21 -> 24, of which waited for: 11 -> 10; matrix products, arithmetic and copies ran while one was open for 1% -> 2% of each run, Pallas kernels for 8% -> 12%
where the time goes in v1:
time: 132 us; the launch traced here: 131 us
  waiting for transfers between devices  49 us (37%)
  starting transfers between devices  48.6 us (37%)
  Pallas kernels  23 us (17%)
  local copies, waits for them, and re-layouts  8.35 us (6%)
    ppermute x18, waiting for transfers between devices, shifted(): lax.ppermute(value, axis, [(i, (i + steps) % count) for i in range(count)])  36.2 us
    ppermute x18, starting transfers between devices, shifted(): lax.ppermute(value, axis, [(i, (i + steps) % count) for i in range(count)])  20.3 us
    all_to_all x1, waiting for transfers between devices, both_halves(): arrived = lax.all_to_all(sent, ZY, split_axis=0, concat_axis=0, tiled=True)  12.9 us
    all_to_all x1, starting transfers between devices, both_halves(): arrived = lax.all_to_all(sent, ZY, split_axis=0, concat_axis=0, tiled=True)  9.5 us
    ppermute x1, starting transfers between devices, from_behind(): lax.ppermute(value, axis, [(source, source + steps) for source in range(l...  7.39 us
    all_to_all x1, starting transfers between devices, both_halves(): back = lax.all_to_all(summed, ZY, split_axis=0, concat_axis=0, tiled=True)  7.34 us
    unnamed x24, local copies, waits for them, and re-layouts  7.03 us
    pallas_call x2, Pallas kernels, near(): pl.pallas_call(functools.partial(near_kernel, shifts), out_shape=sum_shap...  5.54 us
  transfers between devices with their start and end apart: 24, of which 10 were waited for; matrix products, arithmetic and copies ran while one was open for 2% of the time, Pallas kernels for 12%

profile of v1, /device:TPU:1, one launch (start us, length us, event | category | flops | bytes accessed | tf_op | source)
XLA Modules:
  0.0 130.8 jit_solution(474560479303880867)
XLA Ops:
  0.6 3.3 %collective-permute-start.6 = (bf16[2048,512]{1,0:T(8,128)(2,1)}, bf16[2048,512]{1,0:T(8,128)(2,1)}, u32[]{:S(2)}, u32[]{:S(2)}) collective-permute-start(bf16[2048,512]{1,0:T(8,128)(2,1)} %bitcast.9), channel_id=1, source_target_pairs={{0,4},{4,0},{1,5},{5,1},{2,6},{6,2},{3,7},{7,3},{8,12},{12,8},{9,1... | collective-permute-start | bytes 6291464 | tf_op jit(solution)/shard_map/ppermute | solution.py:407
  6.6 1.7 %dispatch_rows.1 = bf16[32,72,128]{2,1,0:T(8,128)(2,1)} custom-call(s32[1]{0:T(128)} %bitcast.part_ref.refs_0_, bf16[256,2048]{1,0:T(8,128)(2,1)S(1)} %copy-done.2, bf16[16,128]{1,0:T(8,128)(2,1)S(1)} %bitcast.19, s32[2,256]{1,0:T(2,128)S(1)} %bitcast.17), custom_call_target="tpu_custom_call" | custom-call | tf_op jit(solution)/shard_map/dispatch_rows/pallas_call | solution.py:397
  8.3 9.5 %all-to-all-start = ((bf16[32,72,128]{2,1,0:T(8,128)(2,1)}), bf16[32,72,128]{2,1,0:T(8,128)(2,1)S(1)}, u32[]{:S(2)}, u32[]{:S(2)}) async-start(bf16[32,72,128]{2,1,0:T(8,128)(2,1)} %dispatch_rows.1), calls=%async_computation | async-start | bytes 1179648 | tf_op jit(solution)/shard_map/all_to_all | solution.py:406
  18.6 1.6 %copy-done.7 = bf16[512,2048]{1,0:T(8,128)(2,1)S(1)} copy-done((bf16[512,2048]{1,0:T(8,128)(2,1)S(1)}, bf16[512,2048]{1,0:T(8,128)(2,1)}, u32[]{:S(2)}) %copy-start.7) | copy-done | bytes 2097176
  22.6 12.9 %all-to-all-done.refs_1_ = bf16[32,72,128]{2,1,0:T(8,128)(2,1)S(1)} async-done(((bf16[32,72,128]{2,1,0:T(8,128)(2,1)}), bf16[32,72,128]{2,1,0:T(8,128)(2,1)S(1)}, u32[]{:S(2)}, u32[]{:S(2)}) %all-to-all-start) | async-done | bytes 589856 | tf_op jit(solution)/shard_map/all_to_all | solution.py:406
  38.3 4.7 %collective-permute-done.refs_1_ = bf16[16,72,128]{2,1,0:T(8,128)(2,1)S(1)} collective-permute-done((bf16[16,72,128]{2,1,0:T(8,128)(2,1)S(1)}, bf16[16,72,128]{2,1,0:T(8,128)(2,1)S(1)}, u32[]{:S(2)}, u32[]{:S(2)}) %collective-permute-start) | collective-permute-done | bytes 294944 | tf_op jit(solution)/shard_map/ppermute | solution.py:22
  43.0 2.7 %collective-permute-start.5 = (bf16[16,72,128]{2,1,0:T(8,128)(2,1)S(1)}, bf16[16,72,128]{2,1,0:T(8,128)(2,1)S(1)}, u32[]{:S(2)}, u32[]{:S(2)}) collective-permute-start(bf16[16,72,128]{2,1,0:T(8,128)(2,1)S(1)} %get-tuple-element.53), channel_id=1, source_target_pairs={{0,3},{1,0},{2,1},{3,2},{4,7},{5,4},{6,5},{7,6},{8,11},{9,8},{10,9... | collective-permute-start | bytes 884744 | tf_op jit(solution)/shard_map/ppermute | solution.py:22
  45.7 2.7 %collective-permute-start.3 = (bf16[16,72,128]{2,1,0:T(8,128)(2,1)S(1)}, bf16[16,72,128]{2,1,0:T(8,128)(2,1)S(1)}, u32[]{:S(2)}, u32[]{:S(2)}) collective-permute-start(bf16[16,72,128]{2,1,0:T(8,128)(2,1)S(1)} %collective-permute-done.2.refs_4_), channel_id=1, source_target_pairs={{0,3},{1,0},{2,1},{3,2},{4,7},{5,4},{6,5},{7,6},{8,11},{9,8},{10,9... | collective-permute-start | bytes 884744 | tf_op jit(solution)/shard_map/ppermute | solution.py:22
  49.9 2.4 %shard_map.140.refs_5_ = f32[4,576,512]{2,1,0:T(8,128)S(1)} custom-call(s32[1]{0:T(128)} %bitcast.part_ref.refs_0_, bf16[32,72,128]{2,1,0:T(8,128)(2,1)S(1)} %all-to-all-done.refs_1_, bf16[2048,512]{1,0:T(8,128)(2,1)S(1)} %bitcast.10, bf16[2048,512]{1,0:T(8,128)(2,1)S(1)} %bitcast.14, bf16[2048,512]{1,0:T(8,128)(2,1)} %collective-permute-done.6.refs_4_.refs_8_.g1_hbm, ...), custom_call_target="tpu_custom_call" | custom-call | flops 1207959552 | bytes 4194304 | tf_op jit(solution)/shard_map/pallas_call | solution.py:443
  52.4 3.1 %shard_map.141.sum_ref = f32[4,576,512]{2,1,0:T(8,128)S(1)} custom-call(s32[1]{0:T(128)} %bitcast.part_ref.refs_0_, bf16[16,72,128]{2,1,0:T(8,128)(2,1)S(1)} %collective-permute-done.refs_1_, bf16[16,72,128]{2,1,0:T(8,128)(2,1)S(1)} %collective-permute-done.4.refs_2_, bf16[16,72,128]{2,1,0:T(8,128)(2,1)S(1)} %collective-permute-done.5.refs_3_, ...), custom_call_target="tpu_custom_call" | custom-call | flops 2415919104 | bytes 4194304 | tf_op jit(solution)/shard_map/pallas_call | solution.py:443
  55.8 4.9 %far_quarter.1 = (bf16[16,72,128]{2,1,0:T(8,128)(2,1)S(1)}, bf16[16,72,128]{2,1,0:T(8,128)(2,1)S(1)}, bf16[576,1024]{1,0:T(8,128)(2,1)S(1)}) custom-call(s32[1]{0:T(128)} %bitcast.part_ref.refs_0_, bf16[16,72,128]{2,1,0:T(8,128)(2,1)S(1)} %collective-permute-done.1.oa_ref, bf16[16,72,128]{2,1,0:T(8,128)(2,1)S(1)} %collective-permute-done.3.ob_ref, ...), custom_call_target="tpu_custom_call" | custom-call | flops 1811939328 | bytes 12582912 | tf_op jit(solution)/shard_map/far_quarter/pallas_call | solution.py:462
  60.8 2.7 %collective-permute-start.11 = (bf16[16,72,128]{2,1,0:T(8,128)(2,1)S(1)}, bf16[16,72,128]{2,1,0:T(8,128)(2,1)S(1)}, u32[]{:S(2)}, u32[]{:S(2)}) collective-permute-start(bf16[16,72,128]{2,1,0:T(8,128)(2,1)S(1)} %get-tuple-element.34), channel_id=1, source_target_pairs={{0,3},{1,0},{2,1},{3,2},{4,7},{5,4},{6,5},{7,6},{8,11},{9,8},{10,9... | collective-permute-start | bytes 884744 | tf_op jit(solution)/shard_map/ppermute | solution.py:22
  63.5 7.4 %collective-permute-start.9 = (bf16[16,256]{1,0:T(8,128)(2,1)S(1)}, bf16[16,256]{1,0:T(8,128)(2,1)S(1)}, u32[]{:S(2)}, u32[]{:S(2)}) collective-permute-start(bf16[16,256]{1,0:T(8,128)(2,1)S(1)} %get-tuple-element.32), channel_id=1, source_target_pairs={{0,4},{4,8},{8,12},{12,16},{16,20},{20,24},{24,28},{28,32},{32,36}... | collective-permute-start | bytes 24584 | tf_op jit(solution)/shard_map/ppermute | solution.py:28
  70.9 4.5 %rest_terms.1 = (bf16[32,72,128]{2,1,0:T(8,128)(2,1)S(1)}, bf16[16,72,128]{2,1,0:T(8,128)(2,1)S(1)}, bf16[16,72,128]{2,1,0:T(8,128)(2,1)S(1)}, bf16[16,72,128]{2,1,0:T(8,128)(2,1)S(1)}, bf16[16,72,128]{2,1,0:T(8,128)(2,1)S(1)}) custom-call(s32[1]{0:T(128)} %bitcast.part_ref.refs_0_, bf16[576,1024]{1,0:T(8,128)(2,1)S(1)} %get-tuple-element.28.hidden_ref, ...), custom_call_target="tpu_custom_call" | custom-call | flops 1811939328 | bytes 8388608 | tf_op jit(solution)/shard_map/rest_terms/pallas_call | solution.py:481
  77.0 2.7 %collective-permute-start.15 = (bf16[16,72,128]{2,1,0:T(8,128)(2,1)S(1)}, bf16[16,72,128]{2,1,0:T(8,128)(2,1)S(1)}, u32[]{:S(2)}, u32[]{:S(2)}) collective-permute-start(bf16[16,72,128]{2,1,0:T(8,128)(2,1)S(1)} %add_convert_fusion), channel_id=1, source_target_pairs={{0,3},{1,0},{2,1},{3,2},{4,7},{5,4},{6,5},{7,6},{8,11},{9,8},{10,9... | collective-permute-start | bytes 884744 | tf_op jit(solution)/shard_map/ppermute | solution.py:22
  81.1 3.4 %collective-permute-done.13.ra_ref = bf16[16,72,128]{2,1,0:T(8,128)(2,1)S(1)} collective-permute-done((bf16[16,72,128]{2,1,0:T(8,128)(2,1)S(1)}, bf16[16,72,128]{2,1,0:T(8,128)(2,1)S(1)}, u32[]{:S(2)}, u32[]{:S(2)}) %collective-permute-start.13) | collective-permute-done | bytes 294944 | tf_op jit(solution)/shard_map/ppermute | solution.py:22
  84.5 2.7 %collective-permute-done.14.lb_ref = bf16[16,72,128]{2,1,0:T(8,128)(2,1)S(1)} collective-permute-done((bf16[16,72,128]{2,1,0:T(8,128)(2,1)S(1)}, bf16[16,72,128]{2,1,0:T(8,128)(2,1)S(1)}, u32[]{:S(2)}, u32[]{:S(2)}) %collective-permute-start.14) | collective-permute-done | bytes 294944 | tf_op jit(solution)/shard_map/ppermute | solution.py:22
  87.1 2.7 %collective-permute-done.15.rb_ref = bf16[16,72,128]{2,1,0:T(8,128)(2,1)S(1)} collective-permute-done((bf16[16,72,128]{2,1,0:T(8,128)(2,1)S(1)}, bf16[16,72,128]{2,1,0:T(8,128)(2,1)S(1)}, u32[]{:S(2)}, u32[]{:S(2)}) %collective-permute-start.15) | collective-permute-done | bytes 294944 | tf_op jit(solution)/shard_map/ppermute | solution.py:22
  89.8 2.7 %collective-permute-done.12.la_ref = bf16[16,72,128]{2,1,0:T(8,128)(2,1)S(1)} collective-permute-done((bf16[16,72,128]{2,1,0:T(8,128)(2,1)}, bf16[16,72,128]{2,1,0:T(8,128)(2,1)S(1)}, u32[]{:S(2)}, u32[]{:S(2)}) %collective-permute-start.12) | collective-permute-done | bytes 294944 | tf_op jit(solution)/shard_map/ppermute | solution.py:22
  93.5 7.3 %all-to-all-start.1 = ((bf16[32,72,128]{2,1,0:T(8,128)(2,1)}), bf16[32,72,128]{2,1,0:T(8,128)(2,1)S(1)}, u32[]{:S(2)}, u32[]{:S(2)}) async-start(bf16[32,72,128]{2,1,0:T(8,128)(2,1)} %ring_sum.1), calls=%async_computation.1 | async-start | bytes 1179648 | tf_op jit(solution)/shard_map/all_to_all | solution.py:527
  103.2 1.8 %collective-permute-start.21 = (bf16[256,512]{1,0:T(8,128)(2,1)S(1)}, bf16[256,512]{1,0:T(8,128)(2,1)S(1)}, u32[]{:S(2)}, u32[]{:S(2)}) collective-permute-start(bf16[256,512]{1,0:T(8,128)(2,1)S(1)} %get-tuple-element.48), channel_id=1, source_target_pairs={{0,3},{1,0},{2,1},{3,2},{4,7},{5,4},{6,5},{7,6},{8,11},{9,8},{10,9... | collective-permute-start | bytes 786440 | tf_op jit(solution)/shard_map/ppermute | solution.py:22
  105.5 1.8 %collective-permute-start.17 = (bf16[512,256]{1,0:T(8,128)(2,1)S(1)}, bf16[512,256]{1,0:T(8,128)(2,1)S(1)}, u32[]{:S(2)}, u32[]{:S(2)}) collective-permute-start(bf16[512,256]{1,0:T(8,128)(2,1)S(1)} %windows.1.refs_0_), channel_id=1, source_target_pairs={{0,2},{1,3},{2,0},{3,1},{4,6},{5,7},{6,4},{7,5},{8,10},{9,11},{10,... | collective-permute-start | bytes 786440 | tf_op jit(solution)/shard_map/ppermute | solution.py:22
  107.3 8.6 %collective-permute-done.19.refs_5_ = bf16[256,512]{1,0:T(8,128)(2,1)S(1)} collective-permute-done((bf16[256,512]{1,0:T(8,128)(2,1)S(1)}, bf16[256,512]{1,0:T(8,128)(2,1)S(1)}, u32[]{:S(2)}, u32[]{:S(2)}) %collective-permute-start.19) | collective-permute-done | bytes 262176 | tf_op jit(solution)/shard_map/ppermute | solution.py:22
  116.8 10.7 %collective-permute-done.16.refs_1_ = bf16[512,256]{1,0:T(8,128)(2,1)S(1)} collective-permute-done((bf16[512,256]{1,0:T(8,128)(2,1)S(1)}, bf16[512,256]{1,0:T(8,128)(2,1)S(1)}, u32[]{:S(2)}, u32[]{:S(2)}) %collective-permute-start.16) | collective-permute-done | bytes 262176 | tf_op jit(solution)/shard_map/ppermute | solution.py:22
  (64 shorter events, 21.6 us)
Async XLA Ops:
  0.6 45.0 %collective-permute-start.6 = (bf16[2048,512]{1,0:T(8,128)(2,1)}, bf16[2048,512]{1,0:T(8,128)(2,1)}, u32[]{:S(2)}, u32[]{:S(2)}) collective-permute-start(bf16[2048,512]{1,0:T(8,128)(2,1)} %bitcast.9), channel_id=1, source_target_pairs={{0,4},{4,0},{1,5},{5,1},{2,6},{6,2},{3,7},{7,3},{8,12},{12,8},{9,1... | collective-permute-start | bytes 6291464 | tf_op jit(solution)/shard_map/ppermute | solution.py:407
  3.9 41.7 %collective-permute-start.7 = (bf16[2048,512]{1,0:T(8,128)(2,1)}, bf16[2048,512]{1,0:T(8,128)(2,1)}, u32[]{:S(2)}, u32[]{:S(2)}) collective-permute-start(bf16[2048,512]{1,0:T(8,128)(2,1)} %bitcast.13), channel_id=1, source_target_pairs={{0,4},{4,0},{1,5},{5,1},{2,6},{6,2},{3,7},{7,3},{8,12},{12,8},{9,1... | collective-permute-start | bytes 6291464 | tf_op jit(solution)/shard_map/ppermute | solution.py:408
  8.3 27.1 %all-to-all-start = ((bf16[32,72,128]{2,1,0:T(8,128)(2,1)}), bf16[32,72,128]{2,1,0:T(8,128)(2,1)S(1)}, u32[]{:S(2)}, u32[]{:S(2)}) async-start(bf16[32,72,128]{2,1,0:T(8,128)(2,1)} %dispatch_rows.1), calls=%async_computation | async-start | bytes 1179648 | tf_op jit(solution)/shard_map/all_to_all | solution.py:406
  17.8 38.0 %collective-permute-start.8 = (bf16[512,2048]{1,0:T(8,128)(2,1)}, bf16[512,2048]{1,0:T(8,128)(2,1)}, u32[]{:S(2)}, u32[]{:S(2)}) collective-permute-start(bf16[512,2048]{1,0:T(8,128)(2,1)} %bitcast.6.d0_ref), channel_id=1, source_target_pairs={{0,4},{4,0},{1,5},{5,1},{2,6},{6,2},{3,7},{7,3},{8,12},{12,8},{9,1... | collective-permute-start | bytes 6291464 | tf_op jit(solution)/shard_map/ppermute | solution.py:409
  35.5 7.5 %collective-permute-start = (bf16[16,72,128]{2,1,0:T(8,128)(2,1)S(1)}, bf16[16,72,128]{2,1,0:T(8,128)(2,1)S(1)}, u32[]{:S(2)}, u32[]{:S(2)}) collective-permute-start(bf16[16,72,128]{2,1,0:T(8,128)(2,1)S(1)} %get-tuple-element.53), channel_id=1, source_target_pairs={{0,1},{1,2},{2,3},{3,0},{4,5},{5,6},{6,7},{7,4},{8,9},{9,10},{10,1... | collective-permute-start | bytes 884744 | tf_op jit(solution)/shard_map/ppermute | solution.py:22
  36.8 6.2 %collective-permute-start.2 = (bf16[16,72,128]{2,1,0:T(8,128)(2,1)S(1)}, bf16[16,72,128]{2,1,0:T(8,128)(2,1)S(1)}, u32[]{:S(2)}, u32[]{:S(2)}) collective-permute-start(bf16[16,72,128]{2,1,0:T(8,128)(2,1)S(1)} %get-tuple-element.52), channel_id=1, source_target_pairs={{0,3},{1,0},{2,1},{3,2},{4,7},{5,4},{6,5},{7,6},{8,11},{9,8},{10,9... | collective-permute-start | bytes 884744 | tf_op jit(solution)/shard_map/ppermute | solution.py:22
  43.0 9.4 %collective-permute-start.4 = (bf16[16,72,128]{2,1,0:T(8,128)(2,1)S(1)}, bf16[16,72,128]{2,1,0:T(8,128)(2,1)S(1)}, u32[]{:S(2)}, u32[]{:S(2)}) collective-permute-start(bf16[16,72,128]{2,1,0:T(8,128)(2,1)S(1)} %get-tuple-element.52), channel_id=1, source_target_pairs={{0,1},{1,2},{2,3},{3,0},{4,5},{5,6},{6,7},{7,4},{8,9},{9,10},{10,1... | collective-permute-start | bytes 884744 | tf_op jit(solution)/shard_map/ppermute | solution.py:22
  43.0 9.4 %collective-permute-start.5 = (bf16[16,72,128]{2,1,0:T(8,128)(2,1)S(1)}, bf16[16,72,128]{2,1,0:T(8,128)(2,1)S(1)}, u32[]{:S(2)}, u32[]{:S(2)}) collective-permute-start(bf16[16,72,128]{2,1,0:T(8,128)(2,1)S(1)} %get-tuple-element.53), channel_id=1, source_target_pairs={{0,3},{1,0},{2,1},{3,2},{4,7},{5,4},{6,5},{7,6},{8,11},{9,8},{10,9... | collective-permute-start | bytes 884744 | tf_op jit(solution)/shard_map/ppermute | solution.py:22
  45.7 10.2 %collective-permute-start.1 = (bf16[16,72,128]{2,1,0:T(8,128)(2,1)S(1)}, bf16[16,72,128]{2,1,0:T(8,128)(2,1)S(1)}, u32[]{:S(2)}, u32[]{:S(2)}) collective-permute-start(bf16[16,72,128]{2,1,0:T(8,128)(2,1)S(1)} %collective-permute-done.refs_1_), channel_id=1, source_target_pairs={{0,1},{1,2},{2,3},{3,0},{4,5},{5,6},{6,7},{7,4},{8,9},{9,10},{10,1... | collective-permute-start | bytes 884744 | tf_op jit(solution)/shard_map/ppermute | solution.py:22
  45.7 10.2 %collective-permute-start.3 = (bf16[16,72,128]{2,1,0:T(8,128)(2,1)S(1)}, bf16[16,72,128]{2,1,0:T(8,128)(2,1)S(1)}, u32[]{:S(2)}, u32[]{:S(2)}) collective-permute-start(bf16[16,72,128]{2,1,0:T(8,128)(2,1)S(1)} %collective-permute-done.2.refs_4_), channel_id=1, source_target_pairs={{0,3},{1,0},{2,1},{3,2},{4,7},{5,4},{6,5},{7,6},{8,11},{9,8},{10,9... | collective-permute-start | bytes 884744 | tf_op jit(solution)/shard_map/ppermute | solution.py:22
  60.7 16.2 %collective-permute-start.10 = (bf16[16,72,128]{2,1,0:T(8,128)(2,1)S(1)}, bf16[16,72,128]{2,1,0:T(8,128)(2,1)S(1)}, u32[]{:S(2)}, u32[]{:S(2)}) collective-permute-start(bf16[16,72,128]{2,1,0:T(8,128)(2,1)S(1)} %get-tuple-element.33), channel_id=1, source_target_pairs={{0,1},{1,2},{2,3},{3,0},{4,5},{5,6},{6,7},{7,4},{8,9},{9,10},{10,1... | collective-permute-start | bytes 884744 | tf_op jit(solution)/shard_map/ppermute | solution.py:22
  60.8 16.1 %collective-permute-start.11 = (bf16[16,72,128]{2,1,0:T(8,128)(2,1)S(1)}, bf16[16,72,128]{2,1,0:T(8,128)(2,1)S(1)}, u32[]{:S(2)}, u32[]{:S(2)}) collective-permute-start(bf16[16,72,128]{2,1,0:T(8,128)(2,1)S(1)} %get-tuple-element.34), channel_id=1, source_target_pairs={{0,3},{1,0},{2,1},{3,2},{4,7},{5,4},{6,5},{7,6},{8,11},{9,8},{10,9... | collective-permute-start | bytes 884744 | tf_op jit(solution)/shard_map/ppermute | solution.py:22
  63.5 13.4 %collective-permute-start.9 = (bf16[16,256]{1,0:T(8,128)(2,1)S(1)}, bf16[16,256]{1,0:T(8,128)(2,1)S(1)}, u32[]{:S(2)}, u32[]{:S(2)}) collective-permute-start(bf16[16,256]{1,0:T(8,128)(2,1)S(1)} %get-tuple-element.32), channel_id=1, source_target_pairs={{0,4},{4,8},{8,12},{12,16},{16,20},{20,24},{24,28},{28,32},{32,36}... | collective-permute-start | bytes 24584 | tf_op jit(solution)/shard_map/ppermute | solution.py:28
  75.4 9.1 %collective-permute-start.13 = (bf16[16,72,128]{2,1,0:T(8,128)(2,1)S(1)}, bf16[16,72,128]{2,1,0:T(8,128)(2,1)S(1)}, u32[]{:S(2)}, u32[]{:S(2)}) collective-permute-start(bf16[16,72,128]{2,1,0:T(8,128)(2,1)S(1)} %get-tuple-element.36), channel_id=1, source_target_pairs={{0,3},{1,0},{2,1},{3,2},{4,7},{5,4},{6,5},{7,6},{8,11},{9,8},{10,9... | collective-permute-start | bytes 884744 | tf_op jit(solution)/shard_map/ppermute | solution.py:22
  76.9 10.2 %collective-permute-start.14 = (bf16[16,72,128]{2,1,0:T(8,128)(2,1)S(1)}, bf16[16,72,128]{2,1,0:T(8,128)(2,1)S(1)}, u32[]{:S(2)}, u32[]{:S(2)}) collective-permute-start(bf16[16,72,128]{2,1,0:T(8,128)(2,1)S(1)} %get-tuple-element.37), channel_id=1, source_target_pairs={{0,1},{1,2},{2,3},{3,0},{4,5},{5,6},{6,7},{7,4},{8,9},{9,10},{10,1... | collective-permute-start | bytes 884744 | tf_op jit(solution)/shard_map/ppermute | solution.py:22
  77.0 12.8 %collective-permute-start.15 = (bf16[16,72,128]{2,1,0:T(8,128)(2,1)S(1)}, bf16[16,72,128]{2,1,0:T(8,128)(2,1)S(1)}, u32[]{:S(2)}, u32[]{:S(2)}) collective-permute-start(bf16[16,72,128]{2,1,0:T(8,128)(2,1)S(1)} %add_convert_fusion), channel_id=1, source_target_pairs={{0,3},{1,0},{2,1},{3,2},{4,7},{5,4},{6,5},{7,6},{8,11},{9,8},{10,9... | collective-permute-start | bytes 884744 | tf_op jit(solution)/shard_map/ppermute | solution.py:22
  80.5 11.9 %collective-permute-start.12 = (bf16[16,72,128]{2,1,0:T(8,128)(2,1)}, bf16[16,72,128]{2,1,0:T(8,128)(2,1)S(1)}, u32[]{:S(2)}, u32[]{:S(2)}) collective-permute-start(bf16[16,72,128]{2,1,0:T(8,128)(2,1)} %add_convert_fusion.1), channel_id=1, source_target_pairs={{0,1},{1,2},{2,3},{3,0},{4,5},{5,6},{6,7},{7,4},{8,9},{9,10},{10,1... | collective-permute-start | bytes 884744 | tf_op jit(solution)/shard_map/ppermute | solution.py:22
  93.5 36.0 %all-to-all-start.1 = ((bf16[32,72,128]{2,1,0:T(8,128)(2,1)}), bf16[32,72,128]{2,1,0:T(8,128)(2,1)S(1)}, u32[]{:S(2)}, u32[]{:S(2)}) async-start(bf16[32,72,128]{2,1,0:T(8,128)(2,1)} %ring_sum.1), calls=%async_computation.1 | async-start | bytes 1179648 | tf_op jit(solution)/shard_map/all_to_all | solution.py:527
  102.2 13.7 %collective-permute-start.19 = (bf16[256,512]{1,0:T(8,128)(2,1)S(1)}, bf16[256,512]{1,0:T(8,128)(2,1)S(1)}, u32[]{:S(2)}, u32[]{:S(2)}) collective-permute-start(bf16[256,512]{1,0:T(8,128)(2,1)S(1)} %get-tuple-element.50), channel_id=1, source_target_pairs={{0,1},{1,2},{2,3},{3,0},{4,5},{5,6},{6,7},{7,4},{8,9},{9,10},{10,1... | collective-permute-start | bytes 786440 | tf_op jit(solution)/shard_map/ppermute | solution.py:22
  102.3 14.5 %collective-permute-start.20 = (bf16[256,512]{1,0:T(8,128)(2,1)S(1)}, bf16[256,512]{1,0:T(8,128)(2,1)S(1)}, u32[]{:S(2)}, u32[]{:S(2)}) collective-permute-start(bf16[256,512]{1,0:T(8,128)(2,1)S(1)} %get-tuple-element.49), channel_id=1, source_target_pairs={{0,2},{1,3},{2,0},{3,1},{4,6},{5,7},{6,4},{7,5},{8,10},{9,11},{10,... | collective-permute-start | bytes 786440 | tf_op jit(solution)/shard_map/ppermute | solution.py:22
  103.2 13.6 %collective-permute-start.21 = (bf16[256,512]{1,0:T(8,128)(2,1)S(1)}, bf16[256,512]{1,0:T(8,128)(2,1)S(1)}, u32[]{:S(2)}, u32[]{:S(2)}) collective-permute-start(bf16[256,512]{1,0:T(8,128)(2,1)S(1)} %get-tuple-element.48), channel_id=1, source_target_pairs={{0,3},{1,0},{2,1},{3,2},{4,7},{5,4},{6,5},{7,6},{8,11},{9,8},{10,9... | collective-permute-start | bytes 786440 | tf_op jit(solution)/shard_map/ppermute | solution.py:22
  104.9 22.6 %collective-permute-start.16 = (bf16[512,256]{1,0:T(8,128)(2,1)S(1)}, bf16[512,256]{1,0:T(8,128)(2,1)S(1)}, u32[]{:S(2)}, u32[]{:S(2)}) collective-permute-start(bf16[512,256]{1,0:T(8,128)(2,1)S(1)} %windows.1.refs_0_), channel_id=1, source_target_pairs={{0,1},{1,2},{2,3},{3,0},{4,5},{5,6},{6,7},{7,4},{8,9},{9,10},{10,1... | collective-permute-start | bytes 786440 | tf_op jit(solution)/shard_map/ppermute | solution.py:22
  105.5 22.0 %collective-permute-start.17 = (bf16[512,256]{1,0:T(8,128)(2,1)S(1)}, bf16[512,256]{1,0:T(8,128)(2,1)S(1)}, u32[]{:S(2)}, u32[]{:S(2)}) collective-permute-start(bf16[512,256]{1,0:T(8,128)(2,1)S(1)} %windows.1.refs_0_), channel_id=1, source_target_pairs={{0,2},{1,3},{2,0},{3,1},{4,6},{5,7},{6,4},{7,5},{8,10},{9,11},{10,... | collective-permute-start | bytes 786440 | tf_op jit(solution)/shard_map/ppermute | solution.py:22
  115.9 12.0 %collective-permute-start.18 = (bf16[512,256]{1,0:T(8,128)(2,1)S(1)}, bf16[512,256]{1,0:T(8,128)(2,1)S(1)}, u32[]{:S(2)}, u32[]{:S(2)}) collective-permute-start(bf16[512,256]{1,0:T(8,128)(2,1)S(1)} %windows.1.refs_0_), channel_id=1, source_target_pairs={{0,3},{1,0},{2,1},{3,2},{4,7},{5,4},{6,5},{7,6},{8,11},{9,8},{10,9... | collective-permute-start | bytes 786440 | tf_op jit(solution)/shard_map/ppermute | solution.py:22
  (12 other events, 116.1 us)
